TPU v7x, 256 devices: a whole 4x4x8 slice. The times are simulated.
256 devices in a mesh: sp: 32 (over z, y), tp: 8 (over x, core).
Axes of the slice: x: 4, y: 4, z: 8, core: 2. Of those that a mesh axis runs over, the one named last changes fastest.
Arguments:
- inputs: bfloat16 [16384, 2048], P('sp', 'tp'), may hold values from -6 to 6
- norm_gain: float32 [2048], replicated, may hold values from 0.1 to 1.9
- latent_query: bfloat16 [2048, 1536], P(None, 'tp'), may hold values from -2 to 2
- latent_down: bfloat16 [2048, 512], replicated, may hold values from -2 to 2
- rope_down: bfloat16 [2048, 32], replicated, may hold values from -2 to 2
- latent_gain: float32 [512], replicated, may hold values from 0.1 to 1.9
- latent_up: bfloat16 [512, 2048], P(None, 'tp'), may hold values from -2 to 2
- window_query: bfloat16 [2048, 1024], P(None, 'tp'), may hold values from -2 to 2
- window_key: bfloat16 [2048, 512], P(None, 'tp'), may hold values from -2 to 2
- window_value: bfloat16 [2048, 512], P(None, 'tp'), may hold values from -0.125 to 0.125
- sink_logit: float32 [16], P('tp'), may hold values from 3 to 8
- out_latent: bfloat16 [1024, 2048], P('tp'), may hold values from -0.1875 to 0.1875
- out_window: bfloat16 [1024, 2048], P('tp'), may hold values from -0.1875 to 0.1875
Outputs:
- attended: bfloat16 [16384, 2048], P('sp', 'tp')
All inputs are finite; a program needn't handle non-finite values.
Results may differ from a plain program's by a relative error of at most 0.017.
Values may be sent and summed in bfloat16 or wider, within the bound.
A program may use at most 128 MiB of HBM per device.

v0:
```python
import jax
import jax.numpy as jnp
from jax import lax
from jax.sharding import PartitionSpec as P

NOPE = 64
ROPE = 32
HEAD = 64
WINDOW = 128


epsilon = 1e-06
key_block = 512


def sent_to_all(value, axis):
    peers = lax.axis_size(axis)
    return lax.all_to_all(
        jnp.broadcast_to(value[None], (peers, *value.shape)), axis, 0, 0, tiled=True
    )


def in_order(parts, dim):
    parts = jnp.moveaxis(parts, 0, dim)
    shape = parts.shape
    return parts.reshape(*shape[:dim], shape[dim] * shape[dim + 1], *shape[dim + 2 :])


def gather_directly(value, axis, dim):
    parts = sent_to_all(value, axis)
    return in_order(parts, dim)


def sent_together(arrays, axis, dim, along):
    ends, at = ([], 0)
    for a in arrays[:-1]:
        at += a.shape[along]
        ends.append(at)
    both = jnp.concatenate(arrays, axis=along)
    return tuple(jnp.split(lax.all_gather(both, axis, axis=dim, tiled=True), ends, axis=along))


def with_halo(cells, sides, width):
    for axis, dim in sides:
        count = lax.axis_size(axis)
        ends = count - 1
        head = lax.slice_in_dim(cells, 0, width, axis=dim)
        tail = lax.slice_in_dim(cells, cells.shape[dim] - width, cells.shape[dim], axis=dim)
        cells = jnp.concatenate(
            [
                lax.ppermute(tail, axis, [(i, (i + 1) % count) for i in range(ends)]),
                cells,
                lax.ppermute(head, axis, [((i + 1) % count, i) for i in range(ends)]),
            ],
            axis=dim,
        )
    return cells


def in_blocks(value, dim, peers):
    shape = value.shape
    parts = value.reshape(*shape[:dim], peers, shape[dim] // peers, *shape[dim + 1 :])
    return jnp.moveaxis(parts, dim, 0)


def summed_on_arrival(value, axis, dim):
    parts = in_blocks(value, dim, lax.axis_size(axis))
    arrived = lax.all_to_all(parts, axis, split_axis=0, concat_axis=0, tiled=True)
    return arrived.astype(jnp.float32).sum(axis=0)


def rms_scale(values, gains):
    return values * lax.rsqrt(jnp.mean(values * values, axis=-1, keepdims=True) + epsilon) * gains


def rotary(values, positions):
    half_width = values.shape[-1] // 2
    inverse = 1.0 / 10000.0 ** (
        jnp.arange(0, 2 * half_width, 2).astype(jnp.float32) / (2 * half_width)
    )
    angles = positions[:, None] * inverse[None, :]
    cosine_table = jnp.cos(angles)[:, None, :]
    sine_table = jnp.sin(angles)[:, None, :]
    first_half = values[..., :half_width]
    second_half = values[..., half_width:]
    return jnp.concatenate(
        [
            first_half * cosine_table - second_half * sine_table,
            second_half * cosine_table + first_half * sine_table,
        ],
        axis=-1,
    )


def attend(running, queries, key_data, rope_keys):
    maxima, denoms, totals = running
    head_count = queries.shape[1]
    stacked = key_data.reshape(key_data.shape[0], head_count, NOPE + HEAD)
    scores = jnp.einsum(
        "qhn,khn->hqk", queries[..., :NOPE], stacked[..., :NOPE], preferred_element_type=jnp.float32
    )
    scores = scores + jnp.einsum(
        "qhr,kr->hqk", queries[..., NOPE:], rope_keys, preferred_element_type=jnp.float32
    )
    scores = scores * (NOPE + ROPE) ** (-0.5)
    highest = jnp.maximum(maxima, jnp.max(scores, axis=-1))
    weights = jnp.exp(scores - highest[..., None])
    shrink = jnp.exp(maxima - highest)
    denoms = denoms * shrink + jnp.sum(weights, axis=-1)
    totals = totals * jnp.transpose(shrink)[:, :, None] + jnp.einsum(
        "hqk,khd->qhd",
        weights.astype(jnp.bfloat16),
        stacked[..., NOPE:],
        preferred_element_type=jnp.float32,
    )
    return (highest, denoms, totals)


def attend_rows(running, queries, key_data, rope_keys):
    row_total = key_data.shape[0]

    def advance(state_now, pieces):
        return (attend(state_now, queries, pieces[0], pieces[1]), None)

    sliced = (
        key_data.reshape(row_total // key_block, key_block, key_data.shape[1]),
        rope_keys.reshape(row_total // key_block, key_block, rope_keys.shape[1]),
    )
    running, unused = lax.scan(advance, running, sliced)
    return running


def shards(
    inputs,
    norm_gain,
    latent_query,
    latent_down,
    rope_down,
    latent_gain,
    latent_up,
    window_query,
    window_key,
    window_value,
    sink_logit,
    out_latent,
    out_window,
):
    row_count = inputs.shape[0]
    gathered = gather_directly(inputs, "tp", 1)
    hidden = rms_scale(gathered.astype(jnp.float32), norm_gain).astype(jnp.bfloat16)
    offset = lax.axis_index("sp") * row_count
    length_all = row_count * lax.axis_size("sp")
    positions = (offset + jnp.arange(row_count)).astype(jnp.float32)
    latent = rms_scale(
        jnp.dot(hidden, latent_down, preferred_element_type=jnp.float32), latent_gain
    ).astype(jnp.bfloat16)
    shared = rotary(
        jnp.dot(hidden, rope_down, preferred_element_type=jnp.float32)[:, None, :], positions
    )[:, 0, :].astype(jnp.bfloat16)
    head_count = latent_up.shape[1] // (NOPE + HEAD)
    queries = jnp.dot(hidden, latent_query, preferred_element_type=jnp.float32).reshape(
        row_count, head_count, NOPE + ROPE
    )
    queries = jnp.concatenate(
        [queries[..., :NOPE], rotary(queries[..., NOPE:], positions)], axis=-1
    ).astype(jnp.bfloat16)
    start_state = (
        jnp.full((head_count, row_count), -jnp.inf, jnp.float32),
        jnp.zeros((head_count, row_count), jnp.float32),
        jnp.zeros((row_count, head_count, HEAD), jnp.float32),
    )
    expanded = jnp.dot(latent, latent_up, preferred_element_type=jnp.float32).astype(jnp.bfloat16)
    pieces = sent_together((expanded, shared), "sp", 0, 1)
    maxima, denoms, totals = attend_rows(start_state, queries, pieces[0], pieces[1])
    latent_out = (
        (totals / jnp.transpose(denoms)[:, :, None])
        .reshape(row_count, head_count * HEAD)
        .astype(jnp.bfloat16)
    )
    window_heads = window_query.shape[1] // HEAD
    key_heads = window_key.shape[1] // HEAD
    group_size = window_heads // key_heads
    window_queries = rotary(
        jnp.dot(hidden, window_query, preferred_element_type=jnp.float32).reshape(
            row_count, window_heads, HEAD
        ),
        positions,
    ).astype(jnp.bfloat16)
    window_keys = rotary(
        jnp.dot(hidden, window_key, preferred_element_type=jnp.float32).reshape(
            row_count, key_heads, HEAD
        ),
        positions,
    ).astype(jnp.bfloat16)
    window_values = jnp.dot(hidden, window_value, preferred_element_type=jnp.float32).astype(
        jnp.bfloat16
    )
    packed = jnp.concatenate(
        [window_keys.reshape(row_count, key_heads * HEAD), window_values], axis=1
    )
    padded = with_halo(packed, (("sp", 0),), WINDOW)
    block_count = row_count // WINDOW
    grid_rows = padded.reshape(block_count + 2, WINDOW, packed.shape[1])
    banded = jnp.concatenate([grid_rows[:-2], grid_rows[1:-1], grid_rows[2:]], axis=1)
    band_keys = banded[..., : key_heads * HEAD].reshape(block_count, 3 * WINDOW, key_heads, HEAD)
    band_values = banded[..., key_heads * HEAD :].reshape(block_count, 3 * WINDOW, key_heads, HEAD)
    query_band = window_queries.reshape(block_count, WINDOW, key_heads, group_size, HEAD)
    scores = jnp.einsum(
        "nqhgd,nkhd->nhgqk", query_band, band_keys, preferred_element_type=jnp.float32
    ) * HEAD ** (-0.5)
    offsets = jnp.arange(3 * WINDOW)[None, :] - jnp.arange(WINDOW)[:, None]
    key_pos = (
        offset
        - WINDOW
        + jnp.arange(block_count)[:, None] * WINDOW
        + jnp.arange(3 * WINDOW)[None, :]
    )
    allowed = ((offsets >= 0) & (offsets <= 2 * WINDOW))[None] & (
        (key_pos >= 0) & (key_pos < length_all)
    )[:, None, :]
    scores = jnp.where(allowed[:, None, None], scores, -jnp.inf)
    sink_table = sink_logit.reshape(key_heads, group_size)[None, :, :, None]
    highest = jnp.maximum(jnp.max(scores, axis=-1), sink_table)
    weights = jnp.exp(scores - highest[..., None])
    denominators = jnp.sum(weights, axis=-1) + jnp.exp(sink_table - highest)
    window_mix = jnp.einsum(
        "nhgqk,nkhd->nqhgd",
        weights.astype(jnp.bfloat16),
        band_values,
        preferred_element_type=jnp.float32,
    )
    window_out = (
        (window_mix / jnp.transpose(denominators, (0, 3, 1, 2))[..., None])
        .reshape(row_count, window_heads * HEAD)
        .astype(jnp.bfloat16)
    )
    contract_dims = (((0,), (1,)), ((), ()))
    own_rows = summed_on_arrival(
        (
            lax.dot_general(
                out_latent, latent_out, contract_dims, preferred_element_type=jnp.float32
            )
            + lax.dot_general(
                out_window, window_out, contract_dims, preferred_element_type=jnp.float32
            )
        ).astype(jnp.bfloat16),
        "tp",
        0,
    )
    return jnp.transpose(own_rows).astype(jnp.bfloat16)


def solution(mesh):
    in_specs = (
        P("sp", "tp"),
        P(),
        P(None, "tp"),
        P(),
        P(),
        P(),
        P(None, "tp"),
        P(None, "tp"),
        P(None, "tp"),
        P(None, "tp"),
        P("tp"),
        P("tp", None),
        P("tp", None),
    )
    out_specs = P("sp", "tp")
    return jax.shard_map(shards, mesh=mesh, in_specs=in_specs, out_specs=out_specs, check_vma=False)
```

profile of v0, /device:TPU:1, one launch (start us, length us, event | category | flops | bytes accessed | tf_op | source)
XLA Modules:
  0.0 310.3 jit_solution(14386173593540342198)
XLA Ops:
  6.5 2.5 broadcast_in_dim.21
  9.1 7.4 %all-to-all-start = ((bf16[8,512,256]{2,1,0:T(8,128)(2,1)}), bf16[8,512,256]{2,1,0:T(8,128)(2,1)}, u32[]{:S(2)}, u32[]{:S(2)}) async-start(bf16[8,512,256]{2,1,0:T(8,128)(2,1)} %broadcast_in_dim.21), calls=%async_computation | async-start | bytes 4194304 | tf_op jit(solution)/shard_map/all_to_all | solution.py:18
  16.5 26.3 %all-to-all-done = bf16[8,512,256]{2,1,0:T(8,128)(2,1)} async-done(((bf16[8,512,256]{2,1,0:T(8,128)(2,1)}), bf16[8,512,256]{2,1,0:T(8,128)(2,1)}, u32[]{:S(2)}, u32[]{:S(2)}) %all-to-all-start) | async-done | bytes 2097184 | tf_op jit(solution)/shard_map/all_to_all | solution.py:18
  42.8 3.9 %copy.48 = bf16[8,512,256]{1,2,0:T(8,128)(2,1)} copy(bf16[8,512,256]{2,1,0:T(8,128)(2,1)} %all-to-all-done) | data formatting | bytes 4194304 | tf_op jit(solution)/shard_map/all_to_all | solution.py:18
  46.8 2.3 multiply_reduce_fusion
  49.0 0.5 fusion.18
  50.4 1.3 multiply_reduce_fusion.1
  52.5 0.7 pad_maximum_fusion
  54.5 0.5 multiply_convert_fusion
  55.0 0.6 copy-done.16
  55.6 0.6 fusion.71
  56.2 1.0 copy-done.3
  58.5 1.3 collective-permute-start.1
  59.8 4.2 %collective-permute-start = (bf16[128,128]{0,1:T(8,128)(2,1)S(1)}, bf16[128,128]{0,1:T(8,128)(2,1)S(1)}, u32[]{:S(2)}, u32[]{:S(2)}) collective-permute-start(bf16[128,128]{0,1:T(8,128)(2,1)S(1)} %get-tuple-element.125), channel_id=1, source_target_pairs={{0,8},{8,16},{16,24},{24,32},{32,40},{40,48},{48,56},{56,64},{64,7... | collective-permute-start | bytes 98312 | tf_op jit(solution)/shard_map/ppermute | solution.py:51
  66.4 91.0 %all-gather.2.cloned.1.call-done = bf16[16384,288]{0,1:T(8,128)(2,1)} async-done(((bf16[512,288]{0,1:T(8,128)(2,1)}), bf16[16384,288]{0,1:T(8,128)(2,1)}) %all-gather.2.cloned.1.call-update) | async-done | bytes 9437200 | tf_op jit(solution)/shard_map/all_gather | solution.py:40
  157.3 7.6 %split.8 = bf16[16384,256]{0,1:T(8,128)(2,1)} slice(bf16[16384,288]{0,1:T(8,128)(2,1)} %all-gather.2.cloned.1.call-done), slice={[0:16384], [0:256]} | slice | bytes 16777216 | tf_op jit(solution)/shard_map/split | solution.py:40
  164.9 7.8 %copy.91 = bf16[32,32,8,512]{3,2,0,1:T(8,128)(2,1)} copy(bf16[32,32,8,512]{3,2,1,0:T(8,128)(2,1)} %bitcast.159) | data formatting | bytes 16777216 | tf_op jit(solution)/shard_map/reshape | solution.py:126
  172.8 1.2 slice-done
  174.1 90.1 %while.15 = (s32[]{:T(128)}, f32[2,512]{1,0:T(2,128)S(1)}, f32[2,512]{1,0:T(2,128)S(1)}, f32[512,2,64]{0,2,1:T(8,128)S(1)}, bf16[32,512,256]{1,2,0:T(8,128)(2,1)...) while((s32[]{:T(128)}, f32[2,512]{1,0:T(2,128)S(1)}, ...), condition=%wide.region_5.6_spmd.clone, body=%wide.region_2.5_spmd.clone.sunk | while | flops 171644928 | bytes 12091513 | solution.py:129
  174.1 1.0 constant_dynamic-slice_fusion.2
  176.1 0.5 fusion.109
  177.0 1.0 constant_dynamic-slice_fusion.2
  179.0 0.5 fusion.109
  179.8 1.0 constant_dynamic-slice_fusion.2
  181.8 0.5 fusion.109
  182.6 1.0 constant_dynamic-slice_fusion.2
  184.6 0.5 fusion.109
  185.4 1.0 constant_dynamic-slice_fusion.2
  188.3 1.0 constant_dynamic-slice_fusion.2
  191.1 1.0 constant_dynamic-slice_fusion.2
  193.9 1.0 constant_dynamic-slice_fusion.2
  196.7 1.0 constant_dynamic-slice_fusion.2
  198.6 0.5 fusion.109
  199.5 1.0 constant_dynamic-slice_fusion.2
  201.5 0.5 fusion.109
  202.3 1.0 constant_dynamic-slice_fusion.2
  205.1 1.0 constant_dynamic-slice_fusion.2
  207.9 1.0 constant_dynamic-slice_fusion.2
  210.8 1.0 constant_dynamic-slice_fusion.2
  213.6 1.0 constant_dynamic-slice_fusion.2
  216.4 1.0 constant_dynamic-slice_fusion.2
  219.2 1.0 constant_dynamic-slice_fusion.2
  222.0 1.0 constant_dynamic-slice_fusion.2
  224.8 1.0 constant_dynamic-slice_fusion.2
  227.6 1.0 constant_dynamic-slice_fusion.2
  230.4 1.0 constant_dynamic-slice_fusion.2
  232.4 0.5 fusion.109
  233.3 1.0 constant_dynamic-slice_fusion.2
  235.2 0.5 fusion.109
  236.1 1.0 constant_dynamic-slice_fusion.2
  238.9 1.0 constant_dynamic-slice_fusion.2
  240.8 0.5 fusion.109
  241.7 1.0 constant_dynamic-slice_fusion.2
  244.5 1.0 constant_dynamic-slice_fusion.2
  247.3 1.0 constant_dynamic-slice_fusion.2
  250.1 1.0 constant_dynamic-slice_fusion.2
  252.9 1.0 constant_dynamic-slice_fusion.2
  255.8 1.0 constant_dynamic-slice_fusion.2
  258.6 1.0 constant_dynamic-slice_fusion.2
  261.4 1.0 constant_dynamic-slice_fusion.2
  264.2 0.7 fusion.72
  265.3 0.7 add_convert_fusion
  266.2 34.7 %all_to_all.10 = bf16[8,256,512]{1,2,0:T(8,128)(2,1)} all-to-all(bf16[8,256,512]{1,2,0:T(8,128)(2,1)S(1)} %bitcast.165), channel_id=1, replica_groups=mesh['sp'=32,'tp'=8] {'tp'}, dimensions={0} | all-to-all | bytes 4194304 | tf_op jit(solution)/shard_map/all_to_all | solution.py:68
  300.8 2.6 reduce_sum.54
  (296 shorter events, 59.5 us)
Async XLA Ops:
  6.5 43.9 %copy-start = (bf16[2048,512]{1,0:T(8,128)(2,1)S(1)}, bf16[2048,512]{1,0:T(8,128)(2,1)}, u32[]{:S(2)}) copy-start(bf16[2048,512]{1,0:T(8,128)(2,1)} %param.18) | copy-start | bytes 6291460
  9.1 33.7 %all-to-all-start = ((bf16[8,512,256]{2,1,0:T(8,128)(2,1)}), bf16[8,512,256]{2,1,0:T(8,128)(2,1)}, u32[]{:S(2)}, u32[]{:S(2)}) async-start(bf16[8,512,256]{2,1,0:T(8,128)(2,1)} %broadcast_in_dim.21), calls=%async_computation | async-start | bytes 4194304 | tf_op jit(solution)/shard_map/all_to_all | solution.py:18
  16.5 140.9 %all-gather.2.cloned.1.call-start = ((), (), s32[]{:S(2)}) async-start(), calls=%async_computation.2 | async-start | bytes 9732096 | tf_op jit(solution)/shard_map/all_gather | solution.py:40
  42.8 6.2 %copy-start.13 = (f32[2048]{0:T(1024)S(1)}, f32[2048]{0:T(1024)}, u32[]{:S(2)}) copy-start(f32[2048]{0:T(1024)} %param.16) | copy-start | bytes 24580
  46.8 2.3 copy-start.4
  49.0 0.9 copy-start.12
  49.9 1.8 copy-start.2
  50.4 1.6 copy-start.11
  50.4 1.6 copy-start.14
  51.8 1.5 copy-start.7
  51.8 2.6 copy-start.5
  54.4 1.1 copy-start.16
  55.6 1.6 copy-start.3
  55.6 1.6 copy-start.9
  56.2 1.9 copy-start.10
  58.5 6.1 %collective-permute-start.1 = (bf16[128,128]{0,1:T(8,128)(2,1)S(1)}, bf16[128,128]{0,1:T(8,128)(2,1)S(1)}, u32[]{:S(2)}, u32[]{:S(2)}) collective-permute-start(bf16[128,128]{0,1:T(8,128)(2,1)S(1)} %get-tuple-element.124), channel_id=1, source_target_pairs={{8,0},{16,8},{24,16},{32,24},{40,32},{48,40},{56,48},{64,56},{72,6... | collective-permute-start | bytes 98312 | tf_op jit(solution)/shard_map/ppermute | solution.py:53
  59.8 5.0 %collective-permute-start = (bf16[128,128]{0,1:T(8,128)(2,1)S(1)}, bf16[128,128]{0,1:T(8,128)(2,1)S(1)}, u32[]{:S(2)}, u32[]{:S(2)}) collective-permute-start(bf16[128,128]{0,1:T(8,128)(2,1)S(1)} %get-tuple-element.125), channel_id=1, source_target_pairs={{0,8},{8,16},{16,24},{24,32},{32,40},{40,48},{48,56},{56,64},{64,7... | collective-permute-start | bytes 98312 | tf_op jit(solution)/shard_map/ppermute | solution.py:51
  64.6 0.9 copy-start.15
  172.7 1.2 slice-start
  174.1 90.1 %copy-start.6 = (bf16[128,2048]{1,0:T(8,128)(2,1)S(1)}, bf16[128,2048]{1,0:T(8,128)(2,1)}, u32[]{:S(2)}) copy-start(bf16[128,2048]{1,0:T(8,128)(2,1)} %param.26) | copy-start | bytes 1572868
  264.2 1.0 copy-start.8
  266.1 37.3 %copy-start.1 = (bf16[2048,512]{1,0:T(8,128)(2,1)S(1)}, bf16[2048,512]{1,0:T(8,128)(2,1)}, u32[]{:S(2)}) copy-start(bf16[2048,512]{1,0:T(8,128)(2,1)} %param.18) | copy-start | bytes 6291460
Sparse Core Ops, SparseCore 0:
  53.3 103.9 all-gather.1
where the time goes:
time: 312 us; the launch traced here: 310 us
  waiting for transfers between devices  117 us (38%)
  local copies, waits for them, and re-layouts  57.4 us (18%)
  matrix products  52.7 us (17%)
  blocking collectives  34.7 us (11%)
  other arithmetic  19.4 us (6%)
  between operations  13.9 us (4%)
  starting transfers between devices  12.9 us (4%)
    all_gather x1, waiting for transfers between devices, sent_together(): lax.all_gather(both, axis, axis=dim, tiled=True)  91 us
    all_to_all x1, blocking collectives, summed_on_arrival(): lax.all_to_all(parts, axis, split_axis=0, concat_axis=0, tiled=True)  34.7 us
    dynamic_slice x32, local copies, waits for them, and re-layouts, attend_rows(): running, unused = lax.scan(advance, running, sliced)  31.1 us
    all_to_all x1, waiting for transfers between devices, sent_to_all(): lax.all_to_all(jnp.broadcast_to(value[None], (peers, *value.shape)), axis...  26.3 us
    dot_general x32, matrix products, attend(): jnp.einsum('hqk,khd->qhd', weights.astype(jnp.bfloat16), stacked[..., NOP...  15.8 us
    dot_general x32, matrix products, attend(): jnp.einsum('qhn,khn->hqk', queries[..., :NOPE], stacked[..., :NOPE], pref...  15.3 us
    dot_general x32, matrix products, attend(): jnp.einsum('qhr,kr->hqk', queries[..., NOPE:], rope_keys, preferred_eleme...  15.1 us
    reduce_sum x32, other arithmetic, attend(): denoms = denoms * shrink + jnp.sum(weights, axis=-1)  9.72 us
  transfers between devices with their start and end apart: 4, of which 3 were waited for; matrix products, arithmetic and copies ran while one was open for 2% of the time, Pallas kernels for 0%

commit v1 on v0

v1 whole, which is shorter than its diff:
```python
import functools

import jax
import jax.numpy as jnp
from jax import lax
from jax.experimental import pallas as pl
from jax.experimental.pallas import tpu as pltpu
from jax.sharding import PartitionSpec as P

NOPE = 64
ROPE = 32
HEAD = 64
WINDOW = 128
LOG2E = 1.4426950408889634

MESH = pl.DeviceIdType.MESH
VMEM_LIMIT = 60 * 2**20
Z, Y = 8, 4
BLK = 512
KV_ROWS = BLK + BLK + BLK // 4
HALF = KV_ROWS // 2
O_ROWS = 2 * HEAD + 16


epsilon = 1e-06


def sent_to_all(value, axis):
    peers = lax.axis_size(axis)
    return lax.all_to_all(
        jnp.broadcast_to(value[None], (peers, *value.shape)), axis, 0, 0, tiled=True
    )


def in_order(parts, dim):
    parts = jnp.moveaxis(parts, 0, dim)
    shape = parts.shape
    return parts.reshape(*shape[:dim], shape[dim] * shape[dim + 1], *shape[dim + 2 :])


def gather_directly(value, axis, dim):
    parts = sent_to_all(value, axis)
    return in_order(parts, dim)


def in_blocks(value, dim, peers):
    shape = value.shape
    parts = value.reshape(*shape[:dim], peers, shape[dim] // peers, *shape[dim + 1 :])
    return jnp.moveaxis(parts, dim, 0)


def summed_on_arrival(value, axis, dim):
    parts = in_blocks(value, dim, lax.axis_size(axis))
    arrived = lax.all_to_all(parts, axis, split_axis=0, concat_axis=0, tiled=True)
    return arrived.astype(jnp.float32).sum(axis=0)


def rms_scale(values, gains):
    return values * lax.rsqrt(jnp.mean(values * values, axis=-1, keepdims=True) + epsilon) * gains


def rotary(values, positions):
    half_width = values.shape[-1] // 2
    inverse = 1.0 / 10000.0 ** (
        jnp.arange(0, 2 * half_width, 2).astype(jnp.float32) / (2 * half_width)
    )
    angles = positions[:, None] * inverse[None, :]
    cosine_table = jnp.cos(angles)[:, None, :]
    sine_table = jnp.sin(angles)[:, None, :]
    first_half = values[..., :half_width]
    second_half = values[..., half_width:]
    return jnp.concatenate(
        [
            first_half * cosine_table - second_half * sine_table,
            second_half * cosine_table + first_half * sine_table,
        ],
        axis=-1,
    )


def at_sp(index):
    return {"sp": index}


def split3(value):
    high = value.astype(jnp.bfloat16)
    rest = value - high.astype(jnp.float32)
    middle = rest.astype(jnp.bfloat16)
    low = (rest - middle.astype(jnp.float32)).astype(jnp.bfloat16)
    return high, middle, low


def window_part(wkv, wq_ref, sink_ref, out_ref, sp, length_all):
    values_t = jnp.transpose(wkv[...].astype(jnp.float32))[HEAD:, :].astype(jnp.bfloat16)
    sinks = sink_ref[0:1, :]
    rows = lax.broadcasted_iota(jnp.int32, (3 * WINDOW, 2 * WINDOW), 0)
    cols = lax.broadcasted_iota(jnp.int32, (3 * WINDOW, 2 * WINDOW), 1)
    gap = rows - cols % WINDOW
    near = (gap >= 0) & (gap <= 2 * WINDOW)
    blank = jnp.zeros((HEAD, WINDOW), jnp.bfloat16)
    for n in range(BLK // WINDOW):
        here = slice(n * WINDOW, (n + 1) * WINDOW)
        keys = wkv[n * WINDOW : (n + 3) * WINDOW, :]
        queries = jnp.concatenate(
            [
                jnp.concatenate([wq_ref[0:HEAD, here], blank], axis=0),
                jnp.concatenate([wq_ref[HEAD : 2 * HEAD, here], blank], axis=0),
            ],
            axis=1,
        )
        scores = jnp.dot(keys, queries, preferred_element_type=jnp.float32)
        place = rows + (sp * BLK + (n - 1) * WINDOW)
        allowed = near & (place >= 0) & (place < length_all)
        scores = jnp.where(allowed, scores, -jnp.inf)
        highest = jnp.maximum(jnp.max(scores, axis=0, keepdims=True), sinks)
        weights = jnp.exp2(scores - highest)
        denominators = jnp.sum(weights, axis=0, keepdims=True) + jnp.exp2(sinks - highest)
        mix = jnp.dot(
            values_t[:, n * WINDOW : (n + 3) * WINDOW],
            weights.astype(jnp.bfloat16),
            preferred_element_type=jnp.float32,
        )
        mix = mix / denominators
        both = jnp.concatenate([mix[:, :WINDOW], mix[:, WINDOW:]], axis=0)
        out_ref[here, 2 * HEAD :] = jnp.transpose(both).astype(jnp.bfloat16)


def attention_kernel(
    length_all,
    kv_ref,
    q_ref,
    wkv_ref,
    wq_ref,
    sink_ref,
    out_ref,
    kvs,
    ropes,
    qraw,
    qpad,
    wkv,
    s0,
    s1,
    now_max,
    now_shrink,
    run_max,
    acc,
    o_out,
    o_in,
    kv_send,
    kv_recv,
    q_send,
    q_recv,
    o_send,
    o_recv,
    w_send,
    w_recv,
):
    sp = lax.axis_index("sp")
    z, y = sp // Y, sp % Y
    up = ((z + 1) % Z) * Y + y
    down = ((z + Z - 1) % Z) * Y + y
    right = z * Y + (y + 1) % Y
    left = z * Y + (y + Y - 1) % Y
    across = z * Y + (y + 2) % Y
    after = (sp + 1) % (Z * Y)
    before = (sp + Z * Y - 1) % (Z * Y)
    barrier = pltpu.get_barrier_semaphore()
    peers = (up, down, right, left, across, after, before)
    for peer in peers:
        pl.semaphore_signal(barrier, inc=1, device_id=at_sp(peer), device_id_type=MESH)
    pl.semaphore_wait(barrier, len(peers))

    def copy(src, dst, send, recv, peer):
        return pltpu.make_async_remote_copy(
            src_ref=src,
            dst_ref=dst,
            send_sem=send,
            recv_sem=recv,
            device_id=at_sp(peer),
            device_id_type=MESH,
        )

    def kv_half(ref, half):
        return ref.at[pl.ds(half * HALF, HALF)]

    def kv_copy(step, half, upward):
        came = 0 if step == 1 else (2 * step - 3 if upward else 2 * step - 2)
        goes = 7 if step == 4 else (2 * step - 1 if upward else 2 * step)
        src = kv_half(kv_ref if step == 1 else kvs.at[came], half)
        slot = 2 * goes + half
        return copy(
            src, kv_half(kvs.at[goes], half), kv_send.at[slot], kv_recv.at[slot], up if upward else down
        )

    q_half = q_ref.shape[0] // 2
    q_right = copy(q_ref, qraw.at[1], q_send.at[0], q_recv.at[0], right)
    q_left = copy(q_ref, qraw.at[2], q_send.at[1], q_recv.at[1], left)
    q_on_right = copy(
        qraw.at[1, pl.ds(0, q_half)], qraw.at[3, pl.ds(0, q_half)], q_send.at[2], q_recv.at[2], right
    )
    q_on_left = copy(
        qraw.at[2, pl.ds(q_half, q_half)], qraw.at[3, pl.ds(q_half, q_half)], q_send.at[3], q_recv.at[3], left
    )
    w_after = copy(
        wkv_ref.at[pl.ds(BLK - WINDOW, WINDOW)], wkv.at[pl.ds(0, WINDOW)], w_send.at[0], w_recv.at[0], after
    )
    w_before = copy(
        wkv_ref.at[pl.ds(0, WINDOW)], wkv.at[pl.ds(BLK + WINDOW, WINDOW)], w_send.at[1], w_recv.at[1], before
    )
    w_after.start()
    w_before.start()
    q_right.start()
    q_left.start()
    for half in range(2):
        kv_copy(1, half, True).start()
        kv_copy(1, half, False).start()

    scores_of = (s0, s1)
    blank = jnp.zeros((NOPE, BLK), jnp.bfloat16)

    def set_queries(g, src):
        qpad[2 * g, 0:NOPE] = src[0:NOPE, :]
        qpad[2 * g, NOPE : 2 * NOPE] = blank
        qpad[2 * g + 1, 0:NOPE] = blank
        qpad[2 * g + 1, NOPE : 2 * NOPE] = src[NOPE : 2 * NOPE, :]
        for h in range(2):
            start = 2 * NOPE + h * ROPE
            qpad[2 * g + h, 2 * NOPE : 2 * NOPE + ROPE] = src[start : start + ROPE, :]
            qpad[2 * g + h, 2 * NOPE + ROPE :] = jnp.zeros((128 - ROPE, BLK), jnp.bfloat16)

    def set_ropes(p, packed):
        wide = packed.astype(jnp.float32)
        ropes[p, 0:128] = packed
        for k in range(1, 4):
            ropes[p, 128 * k : 128 * (k + 1)] = pltpu.roll(wide, 128 - 32 * k, 1).astype(jnp.bfloat16)

    def keys_of(p):
        return jnp.concatenate([kvs[p, 0:BLK, :], ropes[p]], axis=1)

    def scores_stage(p, g, h):
        scores = jnp.dot(keys_of(p), qpad[2 * g + h], preferred_element_type=jnp.float32)
        scores_of[h][...] = scores
        before_max = run_max[2 * g + h]
        highest = jnp.maximum(before_max, jnp.max(scores, axis=0, keepdims=True))
        now_shrink[h] = jnp.exp2(before_max - highest)
        now_max[h] = highest
        run_max[2 * g + h] = highest

    def values_stage(p, g, h):
        weights = jnp.exp2(scores_of[h][...] - now_max[h]).astype(jnp.bfloat16)
        values = jnp.concatenate(
            [kvs[p, pl.ds(BLK + 128 * k + HEAD * h, HEAD), :] for k in range(4)], axis=1
        )
        values = jnp.concatenate([values, jnp.ones((16, BLK), jnp.bfloat16)], axis=0)
        mix = jnp.dot(values, weights, preferred_element_type=jnp.float32)
        acc[2 * g + h] = acc[2 * g + h] * now_shrink[h] + mix

    def finish(g, h):
        total = acc[2 * g + h]
        denominator = total[HEAD : HEAD + 1]
        return total[:HEAD] / denominator, run_max[2 * g + h] + jnp.log2(denominator)

    def o_copy(g):
        peer = (None, left, right, across)[g]
        return copy(o_out.at[g - 1], o_in.at[g - 1], o_send.at[g - 1], o_recv.at[g - 1], peer)

    def send_out(g):
        tails = []
        for h in range(2):
            out, level = finish(g, h)
            o_out[g - 1, HEAD * h : HEAD * (h + 1)] = out.astype(jnp.bfloat16)
            tails += [part.astype(jnp.float32) for part in split3(level)]
        tails.append(jnp.zeros((10, BLK), jnp.float32))
        o_out[g - 1, 2 * HEAD :] = jnp.concatenate(tails, axis=0).astype(jnp.bfloat16)
        o_copy(g).start()

    def unit(u):
        w = u - 3
        v = u - 12
        t = u - 24
        k = t // 2
        p = jnp.where(
            u < 3, 0, jnp.where(u < 9, 1 + w // 3, jnp.where(u < 12, u - 9, jnp.where(u < 24, 3 + v // 4, 6 + t % 2)))
        )
        last = jnp.where(k == 0, 3, jnp.where(k == 3, 0, k))
        g = jnp.where(u < 3, u, jnp.where(u < 9, w % 3, jnp.where(u < 12, 3, jnp.where(u < 24, v % 4, last))))
        return p, g

    run_max[...] = jnp.full(run_max.shape, -1e30, jnp.float32)
    acc[...] = jnp.zeros(acc.shape, jnp.float32)
    kvs[0] = kv_ref[...]
    set_queries(0, q_ref)
    set_ropes(0, kv_ref[2 * BLK :, :])
    wkv[WINDOW : WINDOW + BLK, :] = wkv_ref[...]
    w_after.wait()
    w_before.wait()
    window_part(wkv, wq_ref, sink_ref, out_ref, sp, length_all)
    scores_stage(0, 0, 0)

    def arrive(step, half):
        kv_copy(step, half, True).wait_recv()
        kv_copy(step, half, False).wait_recv()

    def at0():
        q_right.wait_recv()
        q_on_right.start()
        q_left.wait_recv()
        q_on_left.start()
        set_queries(1, qraw.at[1])
        set_queries(2, qraw.at[2])

    def at1():
        arrive(1, 0)
        kv_copy(2, 0, True).start()
        kv_copy(2, 0, False).start()

    def at2():
        arrive(1, 1)
        kv_copy(2, 1, True).start()
        kv_copy(2, 1, False).start()
        set_ropes(1, kvs[1, 2 * BLK :, :])
        set_ropes(2, kvs[2, 2 * BLK :, :])

    def at7():
        arrive(2, 0)
        kv_copy(3, 0, True).start()
        kv_copy(3, 0, False).start()

    def at8():
        q_on_right.wait_recv()
        q_on_left.wait_recv()
        set_queries(3, qraw.at[3])

    def at11():
        arrive(2, 1)
        kv_copy(3, 1, True).start()
        kv_copy(3, 1, False).start()
        set_ropes(3, kvs[3, 2 * BLK :, :])
        set_ropes(4, kvs[4, 2 * BLK :, :])

    def at15():
        arrive(3, 0)
        kv_copy(4, 0, True).start()

    def at19():
        arrive(3, 1)
        kv_copy(4, 1, False).start()
        set_ropes(5, kvs[5, 2 * BLK :, :])
        set_ropes(6, kvs[6, 2 * BLK :, :])

    def at24():
        kv_copy(4, 0, True).wait_recv()
        kv_copy(4, 1, False).wait_recv()
        set_ropes(7, kvs[7, 2 * BLK :, :])

    events = {
        0: at0,
        1: at1,
        2: at2,
        7: at7,
        8: at8,
        11: at11,
        15: at15,
        19: at19,
        24: at24,
        26: lambda: send_out(3),
        28: lambda: send_out(1),
        30: lambda: send_out(2),
    }

    def advance(u, carry):
        for when, event in events.items():
            pl.when(u == when)(event)
        p, g = unit(u)
        p_next, g_next = unit(jnp.minimum(u + 1, 31))
        scores_stage(p, g, 1)
        values_stage(p, g, 0)
        scores_stage(p_next, g_next, 0)
        values_stage(p, g, 1)
        return carry

    lax.fori_loop(0, 32, advance, 0)

    own = [finish(0, h) for h in range(2)]
    for g in range(1, 4):
        o_copy(g).wait_recv()
    merged = []
    for h in range(2):
        outs, levels = [own[h][0]], [own[h][1]]
        for g in range(1, 4):
            block = o_in[g - 1].astype(jnp.float32)
            outs.append(block[HEAD * h : HEAD * (h + 1)])
            row = 2 * HEAD + 3 * h
            levels.append(block[row : row + 1] + block[row + 1 : row + 2] + block[row + 2 : row + 3])
        top = functools.reduce(jnp.maximum, levels)
        shares = [jnp.exp2(level - top) for level in levels]
        total = functools.reduce(jnp.add, shares)
        mixed = functools.reduce(jnp.add, [o * (s / total) for o, s in zip(outs, shares)])
        merged.append(mixed)
    out_ref[:, 0 : 2 * HEAD] = jnp.transpose(jnp.concatenate(merged, axis=0)).astype(jnp.bfloat16)

    w_sends = [w_after, w_before, q_right, q_left, q_on_right, q_on_left]
    for step in range(1, 4):
        for half in range(2):
            w_sends += [kv_copy(step, half, True), kv_copy(step, half, False)]
    w_sends += [kv_copy(4, 0, True), kv_copy(4, 1, False)]
    w_sends += [o_copy(g) for g in range(1, 4)]
    for sent in w_sends[2:]:
        sent.wait_send()


def attention(kv, q, wkv, wq, sinks, length_all):
    dma = pltpu.SemaphoreType.DMA
    return pl.pallas_call(
        functools.partial(attention_kernel, length_all),
        out_shape=jax.ShapeDtypeStruct((BLK, 4 * HEAD), jnp.bfloat16),
        in_specs=[pl.BlockSpec(memory_space=pltpu.VMEM)] * 5,
        out_specs=pl.BlockSpec(memory_space=pltpu.VMEM),
        scratch_shapes=[
            pltpu.VMEM((Z, KV_ROWS, 128), jnp.bfloat16),
            pltpu.VMEM((Z, BLK, 128), jnp.bfloat16),
            pltpu.VMEM((Y, 2 * (NOPE + ROPE), BLK), jnp.bfloat16),
            pltpu.VMEM((2 * Y, 256, BLK), jnp.bfloat16),
            pltpu.VMEM((BLK + 2 * WINDOW, 128), jnp.bfloat16),
            pltpu.VMEM((BLK, BLK), jnp.float32),
            pltpu.VMEM((BLK, BLK), jnp.float32),
            pltpu.VMEM((2, 1, BLK), jnp.float32),
            pltpu.VMEM((2, 1, BLK), jnp.float32),
            pltpu.VMEM((2 * Y, 1, BLK), jnp.float32),
            pltpu.VMEM((2 * Y, HEAD + 16, BLK), jnp.float32),
            pltpu.VMEM((Y - 1, O_ROWS, BLK), jnp.bfloat16),
            pltpu.VMEM((Y - 1, O_ROWS, BLK), jnp.bfloat16),
            dma((16,)),
            dma((16,)),
            dma((4,)),
            dma((4,)),
            dma((3,)),
            dma((3,)),
            dma((2,)),
            dma((2,)),
        ],
        compiler_params=pltpu.CompilerParams(
            collective_id=1, has_side_effects=True, vmem_limit_bytes=VMEM_LIMIT
        ),
        name="attention",
    )(kv, q, wkv, wq, sinks)


def shards(
    inputs,
    norm_gain,
    latent_query,
    latent_down,
    rope_down,
    latent_gain,
    latent_up,
    window_query,
    window_key,
    window_value,
    sink_logit,
    out_latent,
    out_window,
):
    row_count = inputs.shape[0]
    gathered = gather_directly(inputs, "tp", 1)
    hidden = rms_scale(gathered.astype(jnp.float32), norm_gain).astype(jnp.bfloat16)
    offset = lax.axis_index("sp") * row_count
    length_all = row_count * lax.axis_size("sp")
    positions = (offset + jnp.arange(row_count)).astype(jnp.float32)
    latent = rms_scale(
        jnp.dot(hidden, latent_down, preferred_element_type=jnp.float32), latent_gain
    ).astype(jnp.bfloat16)
    shared = rotary(
        jnp.dot(hidden, rope_down, preferred_element_type=jnp.float32)[:, None, :], positions
    )[:, 0, :].astype(jnp.bfloat16)
    head_count = latent_up.shape[1] // (NOPE + HEAD)
    queries = jnp.dot(hidden, latent_query, preferred_element_type=jnp.float32).reshape(
        row_count, head_count, NOPE + ROPE
    )
    scale = LOG2E * (NOPE + ROPE) ** (-0.5)
    turned = rotary(queries[..., NOPE:], positions)
    queries_t = (
        jnp.concatenate(
            [
                queries[..., :NOPE].reshape(row_count, head_count * NOPE),
                turned.reshape(row_count, head_count * ROPE),
            ],
            axis=1,
        )
        * scale
    ).T.astype(jnp.bfloat16)
    raising = latent_up.reshape(latent_up.shape[0], head_count, NOPE + HEAD)
    raise_keys = raising[..., :NOPE].reshape(-1, head_count * NOPE)
    raise_values = raising[..., NOPE:].reshape(-1, head_count * HEAD)
    keys = jnp.dot(latent, raise_keys, preferred_element_type=jnp.float32).astype(jnp.bfloat16)
    values_t = lax.dot_general(
        raise_values, latent, (((0,), (1,)), ((), ())), preferred_element_type=jnp.float32
    ).astype(jnp.bfloat16)
    values_t = jnp.swapaxes(values_t.reshape(128, 4, 128), 0, 1).reshape(512, 128)
    packed_rope = jnp.swapaxes(shared.reshape(4, 128, ROPE), 0, 1).reshape(128, 128)
    kv = jnp.concatenate([keys, values_t, packed_rope], axis=0)
    window_heads = window_query.shape[1] // HEAD
    key_heads = window_key.shape[1] // HEAD
    window_queries = rotary(
        jnp.dot(hidden, window_query, preferred_element_type=jnp.float32).reshape(
            row_count, window_heads, HEAD
        ),
        positions,
    )
    queries_w = (
        (window_queries * (LOG2E * HEAD ** (-0.5))).reshape(row_count, window_heads * HEAD).T
    ).astype(jnp.bfloat16)
    window_keys = rotary(
        jnp.dot(hidden, window_key, preferred_element_type=jnp.float32).reshape(
            row_count, key_heads, HEAD
        ),
        positions,
    ).astype(jnp.bfloat16)
    window_values = jnp.dot(hidden, window_value, preferred_element_type=jnp.float32).astype(
        jnp.bfloat16
    )
    packed = jnp.concatenate(
        [window_keys.reshape(row_count, key_heads * HEAD), window_values], axis=1
    )
    sinks = jnp.repeat(sink_logit * LOG2E, WINDOW)[None, :]
    mixed = attention(kv, queries_t, packed, queries_w, sinks, length_all)
    contract_dims = (((0,), (1,)), ((), ()))
    own_rows = summed_on_arrival(
        lax.dot_general(
            jnp.concatenate([out_latent, out_window], axis=0),
            mixed,
            contract_dims,
            preferred_element_type=jnp.float32,
        ).astype(jnp.bfloat16),
        "tp",
        0,
    )
    return jnp.transpose(own_rows).astype(jnp.bfloat16)


def solution(mesh):
    in_specs = (
        P("sp", "tp"),
        P(),
        P(None, "tp"),
        P(),
        P(),
        P(),
        P(None, "tp"),
        P(None, "tp"),
        P(None, "tp"),
        P(None, "tp"),
        P("tp"),
        P("tp", None),
        P("tp", None),
    )
    out_specs = P("sp", "tp")
    return jax.shard_map(shards, mesh=mesh, in_specs=in_specs, out_specs=out_specs, check_vma=False)
```

time: 312 us -> 145 us (0.46)
  waiting for transfers between devices: 117 us -> 22.7 us
  Pallas kernels: 0 us -> 43.8 us
  local copies, waits for them, and re-layouts: 57.4 us -> 13.6 us
  matrix products: 52.7 us -> 10.7 us
  between operations: 13.9 us -> 0.42 us
  other arithmetic: 19.4 us -> 13.8 us
  starting transfers between devices: 12.9 us -> 7.56 us
    all_gather x1 -> x0, waiting for transfers between devices: 91 us -> none  [sent_together(): lax.all_gather(both, axis, axis=dim, tiled=True)]
    dot_general x101 -> x3, matrix products: 48.9 us -> 3.34 us  [the longest x1 1.71 us: shards(): lax.dot_general(jnp.concatenate([out_latent, out_window], axis=0), mixed,...]
    pallas_call x0 -> x1, Pallas kernels: none -> 43.8 us  [attention(): pl.pallas_call(functools.partial(attention_kernel, length_all), out_shape...]
    dynamic_slice x32 -> x0, local copies, waits for them, and re-layouts: 31.1 us -> none  [attend_rows(): running, unused = lax.scan(advance, running, sliced)]
    reduce_sum x33 -> x0, other arithmetic: 9.95 us -> none  [the longest x32 9.72 us: attend(): denoms = denoms * shrink + jnp.sum(weights, axis=-1)]
    split x3 -> x0, local copies, waits for them, and re-layouts: 8.82 us -> none  [sent_together(): jnp.split(lax.all_gather(both, axis, axis=dim, tiled=True), ends, axis=al...]
    reshape x3 -> x2, local copies, waits for them, and re-layouts: 8.07 us -> 0.84 us  [the longest x1 0.71 us: shards(): jnp.swapaxes(shared.reshape(4, 128, ROPE), 0, 1).reshape(128, 128)]
    ppermute x2 -> x0, starting transfers between devices: 5.46 us -> none  [the longest x1 4.17 us: with_halo(): lax.ppermute(tail, axis, [(i, (i + 1) % count) for i in range(ends)])]
  transfers between devices with their start and end apart: 4 -> 1, of which waited for: 3 -> 1; matrix products, arithmetic and copies ran while one was open for 2% -> 2% of each run, Pallas kernels for 0% -> 0%
where the time goes in v1:
time: 145 us
  Pallas kernels  43.8 us (30%)
  blocking collectives  32.3 us (22%)
  waiting for transfers between devices  22.7 us (16%)
  other arithmetic  13.8 us (10%)
  local copies, waits for them, and re-layouts  13.6 us (9%)
  matrix products  10.7 us (7%)
  starting transfers between devices  7.56 us (5%)
    pallas_call x1, Pallas kernels, attention(): pl.pallas_call(functools.partial(attention_kernel, length_all), out_shape...  43.8 us
    all_to_all x1, blocking collectives, summed_on_arrival(): lax.all_to_all(parts, axis, split_axis=0, concat_axis=0, tiled=True)  32.3 us
    all_to_all x1, waiting for transfers between devices, sent_to_all(): lax.all_to_all(jnp.broadcast_to(value[None], (peers, *value.shape)), axis...  22.7 us
    all_to_all x1, starting transfers between devices, sent_to_all(): lax.all_to_all(jnp.broadcast_to(value[None], (peers, *value.shape)), axis...  7.56 us
    unnamed x54, local copies, waits for them, and re-layouts  4.67 us
    all_to_all x1, local copies, waits for them, and re-layouts, sent_to_all(): lax.all_to_all(jnp.broadcast_to(value[None], (peers, *value.shape)), axis...  3.91 us
    dot_general x1, matrix products, shards(): jnp.dot(hidden, latent_down, preferred_element_type=jnp.float32)  2.91 us
  transfers between devices with their start and end apart: 1, of which 1 were waited for; matrix products, arithmetic and copies ran while one was open for 2% of the time, Pallas kernels for 0%

profile of v1, /device:TPU:1, one launch (start us, length us, event | category | flops | bytes accessed | tf_op | source)
XLA Modules:
  0.0 144.8 jit_solution(3607547362248787387)
XLA Ops:
  0.0 0.0 copy-start
  0.0 2.5 %broadcast_in_dim.6 = bf16[8,512,256]{2,1,0:T(8,128)(2,1)} broadcast(bf16[512,256]{1,0:T(8,128)(2,1)} %param.13), dimensions={1,2} | broadcast | bytes 2359296 | tf_op jit(solution)/shard_map/broadcast_in_dim | solution.py:31
  2.5 7.6 %all-to-all-start = ((bf16[8,512,256]{2,1,0:T(8,128)(2,1)}), bf16[8,512,256]{2,1,0:T(8,128)(2,1)}, u32[]{:S(2)}, u32[]{:S(2)}) async-start(bf16[8,512,256]{2,1,0:T(8,128)(2,1)} %broadcast_in_dim.6), calls=%async_computation | async-start | bytes 4194304 | tf_op jit(solution)/shard_map/all_to_all | solution.py:30
  10.1 0.0 copy-done.13
  10.1 0.1 copy.44
  10.3 0.0 copy-done.18
  10.3 0.0 copy-done.6
  10.3 1.0 copy.52
  11.3 0.0 copy-done.24
  11.3 0.6 broadcast_multiply_fusion
  11.9 0.8 multiply_cosine_fusion.2
  12.8 1.0 multiply_cosine_fusion.1
  13.8 22.7 %all-to-all-done = bf16[8,512,256]{2,1,0:T(8,128)(2,1)} async-done(((bf16[8,512,256]{2,1,0:T(8,128)(2,1)}), bf16[8,512,256]{2,1,0:T(8,128)(2,1)}, u32[]{:S(2)}, u32[]{:S(2)}) %all-to-all-start) | async-done | bytes 2097184 | tf_op jit(solution)/shard_map/all_to_all | solution.py:30
  36.4 3.9 %copy.43 = bf16[8,512,256]{1,2,0:T(8,128)(2,1)} copy(bf16[8,512,256]{2,1,0:T(8,128)(2,1)} %all-to-all-done) | data formatting | bytes 4194304 | tf_op jit(solution)/shard_map/all_to_all | solution.py:30
  40.4 2.3 %multiply_reduce_fusion = f32[512]{0:T(512)S(1)} fusion(bf16[8,512,256]{1,2,0:T(8,128)(2,1)} %copy.43), kind=kLoop, calls=%fused_computation.4 | loop fusion | flops 3145216 | bytes 2099200 | tf_op jit(solution)/shard_map/reduce_sum | solution.py:59
  42.6 0.0 copy-done.1
  42.6 0.0 copy-start.14
  42.6 0.5 fusion.1
  43.2 1.3 copy-done.2
  44.5 0.4 convolution_bitcast_fusion.1
  45.0 0.2 fusion.23
  45.2 0.7 copy.47
  45.9 0.0 copy-done
  45.9 2.9 %multiply_reduce_fusion.1 = (f32[512]{0:T(512)S(1)}, f32[512,512]{0,1:T(8,128)S(1)}) fusion(bf16[512,2048]{0,1:T(8,128)(2,1)} %copy-done.2, bf16[2048,512]{1,0:T(8,128)(2,1)S(1)} %copy-done), kind=kOutput, calls=%fused_computation.15 | convolution fusion | flops 1074265600 | bytes 5244928 | tf_op jit(solution)/shard_map/dot_general | solution.py:471
  48.9 0.0 copy-start.19
  48.9 0.0 copy-done.20
  48.9 0.5 convolution_convert_fusion.1
  49.4 0.1 copy-done.19
  49.5 0.1 copy.45
  49.6 1.2 convolution_convert_fusion.2
  50.8 0.0 copy-start.23
  50.8 2.2 %multiply_convert_fusion = bf16[8,512,256]{1,2,0:T(8,128)(2,1)S(1)} fusion(bf16[8,512,256]{1,2,0:T(8,128)(2,1)} %copy.43, f32[8,256]{1,0:T(8,128)S(1)} %mul.277, f32[512]{0:T(512)S(1)} %add_rsqrt_fusion.1), kind=kLoop, calls=%fused_computation.3 | loop fusion | flops 4194304 | bytes 4204544 | tf_op jit(solution)/shard_map/convert.7
  53.0 0.0 copy-start.4
  53.0 0.0 copy-done.23
  53.0 0.0 copy-start.3
  53.0 0.0 copy-start.10
  53.0 0.6 fusion.28
  53.6 0.7 copy-done.4
  54.3 1.1 copy-done.3
  55.3 0.5 convolution_convert_fusion.3
  55.8 0.0 copy-start.22
  55.8 0.1 copy.51
  56.0 2.5 %convolution_bitcast_fusion = f32[512,1,64]{2,0,1:T(8,128)S(1)} fusion(bf16[512,2048]{0,1:T(8,128)(2,1)} %copy-done.2, bf16[2048,64]{0,1:T(8,128)(2,1)} %param.21), kind=kOutput, calls=%fused_computation.6 | convolution fusion | flops 134217728 | bytes 2490368 | tf_op jit(solution)/shard_map/dot_general | solution.py:514
  58.5 0.0 copy-done.22
  58.5 1.2 fusion.17
  59.7 0.0 copy-done.5
  59.7 0.0 copy-done.7
  59.7 0.0 copy-start.15
  59.8 0.4 fusion.29
  60.2 0.2 copy-done.15
  60.5 0.0 copy-done.16
  60.5 0.0 copy-start.8
  60.5 0.0 copy-start.9
  60.6 0.7 fusion.15.q_ref
  61.3 0.0 copy-done.12
  61.3 0.7 fusion.14
  62.0 0.7 pad_maximum_fusion.kv_ref
  62.7 0.8 pad_maximum_fusion.2.wkv_ref
  63.5 0.7 broadcast_in_dim.8
  64.2 43.8 %attention.1 = bf16[512,256]{1,0:T(8,128)(2,1)} custom-call(bf16[1152,128]{1,0:T(8,128)(2,1)} %pad_maximum_fusion.kv_ref, bf16[192,512]{1,0:T(8,128)(2,1)} %fusion.15.q_ref, bf16[512,128]{1,0:T(8,128)(2,1)} %pad_maximum_fusion.2.wkv_ref, bf16[128,512]{1,0:T(8,128)(2,1)} %bitcast.73, f32[1,256]{1,0:T(1,128)} %bitcast.81), custom_call_target="tpu_custom_call" | custom-call | tf_op jit(solution)/shard_map/attention/pallas_call | solution.py:414
  108.0 1.7 %convolution_convert_fusion = bf16[2048,512]{1,0:T(8,128)(2,1)S(1)} fusion(bf16[512,256]{1,0:T(8,128)(2,1)} %attention.1, bf16[128,2048]{1,0:T(8,128)(2,1)S(1)} %copy-done.8, bf16[128,2048]{1,0:T(8,128)(2,1)S(1)} %copy-done.9), kind=kOutput, calls=%fused_computation.5 | convolution fusion | flops 540016640 | bytes 3407872 | tf_op jit(solution)/shard_map/dot_general | solution.py:529
  109.7 32.3 %all_to_all.10 = bf16[8,256,512]{2,1,0:T(8,128)(2,1)} all-to-all(bf16[8,256,512]{2,1,0:T(8,128)(2,1)S(1)} %bitcast.67), channel_id=1, replica_groups=mesh['sp'=32,'tp'=8] {'tp'}, dimensions={0} | all-to-all | bytes 4194304 | tf_op jit(solution)/shard_map/all_to_all | solution.py:54
  142.0 2.0 %reduce_sum.32 = bf16[256,512]{1,0:T(8,128)(2,1)S(1)} reduce(bf16[8,256,512]{2,1,0:T(8,128)(2,1)} %all_to_all.10, bf16[]{:T(256)} %constant.39.clone.1), dimensions={0}, to_apply=%region_2.0 | reduce | flops 917504 | bytes 2359298 | tf_op jit(solution)/shard_map/reduce_sum | solution.py:55
  143.9 0.8 copy.54
  (37 shorter events, 0.2 us)
Async XLA Ops:
  0.0 45.9 %copy-start = (bf16[2048,512]{1,0:T(8,128)(2,1)S(1)}, bf16[2048,512]{1,0:T(8,128)(2,1)}, u32[]{:S(2)}) copy-start(bf16[2048,512]{1,0:T(8,128)(2,1)} %param.16) | copy-start | bytes 6291460
  2.5 7.6 %copy-start.13 = (bf16[512,256]{1,0:T(8,128)(2,1)S(1)}, bf16[512,256]{1,0:T(8,128)(2,1)}, u32[]{:S(2)}) copy-start(bf16[512,256]{1,0:T(8,128)(2,1)} %param.19) | copy-start | bytes 786436
  2.5 7.7 %copy-start.18 = (f32[2048]{0:T(1024)S(1)}, f32[2048]{0:T(1024)}, u32[]{:S(2)}) copy-start(f32[2048]{0:T(1024)} %param.14) | copy-start | bytes 24580
  2.5 7.7 %copy-start.6 = (bf16[2048,128]{1,0:T(8,128)(2,1)S(1)}, bf16[2048,128]{1,0:T(8,128)(2,1)}, u32[]{:S(2)}) copy-start(bf16[2048,128]{1,0:T(8,128)(2,1)} %param.20) | copy-start | bytes 1572868
  2.5 8.8 %copy-start.24 = (f32[2]{0:T(128)S(1)}, f32[2]{0:T(128)}, u32[]{:S(2)}) copy-start(f32[2]{0:T(128)} %param.23) | copy-start | bytes 28
  2.5 33.9 %all-to-all-start = ((bf16[8,512,256]{2,1,0:T(8,128)(2,1)}), bf16[8,512,256]{2,1,0:T(8,128)(2,1)}, u32[]{:S(2)}, u32[]{:S(2)}) async-start(bf16[8,512,256]{2,1,0:T(8,128)(2,1)} %broadcast_in_dim.6), calls=%async_computation | async-start | bytes 4194304 | tf_op jit(solution)/shard_map/all_to_all | solution.py:30
  11.3 25.1 %copy-start.21 = (f32[32]{0:T(128)}, f32[32]{0:T(128)S(1)}, u32[]{:S(2)}) copy-start(f32[32]{0:T(128)S(1)} %negate_power_fusion) | copy-start | bytes 388
  40.4 2.3 %copy-start.1 = (bf16[8,512,256]{1,2,0:T(8,128)(2,1)S(1)}, bf16[8,512,256]{1,2,0:T(8,128)(2,1)}, u32[]{:S(2)}) copy-start(bf16[8,512,256]{1,2,0:T(8,128)(2,1)} %copy.43) | copy-start | bytes 6291460
  42.6 1.9 %copy-start.14 = (bf16[2048,32]{0,1:T(8,128)(2,1)S(1)}, bf16[2048,32]{0,1:T(8,128)(2,1)}, u32[]{:S(2)}) copy-start(bf16[2048,32]{0,1:T(8,128)(2,1)} %param.17) | copy-start | bytes 393220
  43.2 1.3 copy-start.2
  45.9 2.9 %copy-start.20 = (f32[512]{0:T(512)S(1)}, f32[512]{0:T(512)}, u32[]{:S(2)}) copy-start(f32[512]{0:T(512)} %param.18) | copy-start | bytes 6148
  48.9 0.6 copy-start.19
  50.8 2.2 %copy-start.23 = (bf16[2048,192]{0,1:T(8,128)(2,1)S(1)}, bf16[2048,192]{0,1:T(8,128)(2,1)}, u32[]{:S(2)}) copy-start(bf16[2048,192]{0,1:T(8,128)(2,1)} %param.15) | copy-start | bytes 2359300
  53.0 1.3 copy-start.4
  53.0 2.3 %copy-start.3 = (bf16[512,2048]{0,1:T(8,128)(2,1)S(1)}, bf16[512,2048]{0,1:T(8,128)(2,1)}, u32[]{:S(2)}) copy-start(bf16[512,2048]{0,1:T(8,128)(2,1)} %copy-done.2) | copy-start | bytes 6291460
  53.0 2.3 %copy-start.10 = (bf16[2048,64]{0,1:T(8,128)(2,1)S(1)}, bf16[2048,64]{0,1:T(8,128)(2,1)}, u32[]{:S(2)}) copy-start(bf16[2048,64]{0,1:T(8,128)(2,1)} %param.22) | copy-start | bytes 786436
  55.8 2.6 %copy-start.22 = (f32[32]{0:T(128)S(1)}, f32[32]{0:T(128)}, u32[]{:S(2)}) copy-start(f32[32]{0:T(128)} %copy-done.21) | copy-start | bytes 388
  56.0 3.8 %copy-start.5 = (bf16[8,512,256]{1,2,0:T(8,128)(2,1)S(1)}, bf16[8,512,256]{1,2,0:T(8,128)(2,1)}, u32[]{:S(2)}) copy-start(bf16[8,512,256]{1,2,0:T(8,128)(2,1)} %copy-done.4) | copy-start | bytes 6291460
  56.0 3.8 %copy-start.7 = (bf16[2048,128]{0,1:T(8,128)(2,1)S(1)}, bf16[2048,128]{0,1:T(8,128)(2,1)}, u32[]{:S(2)}) copy-start(bf16[2048,128]{0,1:T(8,128)(2,1)} %copy.52) | copy-start | bytes 1572868
  59.7 0.8 copy-start.15
  59.7 0.8 copy-start.16
  59.8 1.5 %copy-start.11 = (f32[512,32]{0,1:T(8,128)S(1)}, f32[512,32]{0,1:T(8,128)}, u32[]{:S(2)}) copy-start(f32[512,32]{0,1:T(8,128)} %get-tuple-element.15) | copy-start | bytes 196612
  59.8 1.5 %copy-start.12 = (f32[512,32]{0,1:T(8,128)S(1)}, f32[512,32]{0,1:T(8,128)}, u32[]{:S(2)}) copy-start(f32[512,32]{0,1:T(8,128)} %get-tuple-element.16) | copy-start | bytes 196612
  60.2 1.8 %copy-start.17 = (bf16[128,128]{1,0:T(8,128)(2,1)S(1)}, bf16[128,128]{1,0:T(8,128)(2,1)}, u32[]{:S(2)}) copy-start(bf16[128,128]{1,0:T(8,128)(2,1)} %copy.47) | copy-start | bytes 98308
  60.2 3.3 %copy-start.25 = (f32[2]{0:T(128)S(1)}, f32[2]{0:T(128)}, u32[]{:S(2)}) copy-start(f32[2]{0:T(128)} %broadcast_multiply_fusion) | copy-start | bytes 28
  60.5 47.4 %copy-start.8 = (bf16[128,2048]{1,0:T(8,128)(2,1)S(1)}, bf16[128,2048]{1,0:T(8,128)(2,1)}, u32[]{:S(2)}) copy-start(bf16[128,2048]{1,0:T(8,128)(2,1)} %param.25) | copy-start | bytes 1572868
  60.5 47.4 %copy-start.9 = (bf16[128,2048]{1,0:T(8,128)(2,1)S(1)}, bf16[128,2048]{1,0:T(8,128)(2,1)}, u32[]{:S(2)}) copy-start(bf16[128,2048]{1,0:T(8,128)(2,1)} %param.24) | copy-start | bytes 1572868

commit v2 on v1

v2 whole, which is shorter than its diff:
```python
import functools

import jax
import jax.numpy as jnp
import numpy as np
from jax import lax
from jax.experimental import pallas as pl
from jax.experimental.pallas import tpu as pltpu
from jax.sharding import PartitionSpec as P

NOPE = 64
ROPE = 32
HEAD = 64
WINDOW = 128
LOG2E = 1.4426950408889634

MESH = pl.DeviceIdType.MESH
VMEM_LIMIT = 60 * 2**20
Z, Y, X = 8, 4, 4
BLK = 512
KV_ROWS = BLK + BLK + BLK // 4
HALF = KV_ROWS // 2
O_ROWS = 2 * HEAD + 16
COLS = 256
ROWS = BLK // 2


epsilon = 1e-06


def at_sp(index):
    return {"sp": index}


def split3(value):
    high = value.astype(jnp.bfloat16)
    rest = value - high.astype(jnp.float32)
    middle = rest.astype(jnp.bfloat16)
    low = (rest - middle.astype(jnp.float32)).astype(jnp.bfloat16)
    return high, middle, low


def window_part(wkv, wq_ref, sink_ref, out_ref, sp, length_all):
    values_t = jnp.transpose(wkv[...].astype(jnp.float32))[HEAD:, :].astype(jnp.bfloat16)
    lane = lax.broadcasted_iota(jnp.int32, (1, 2 * WINDOW), 1)
    sinks = jnp.where(lane < WINDOW, sink_ref[0], sink_ref[1]) * LOG2E
    rows = lax.broadcasted_iota(jnp.int32, (3 * WINDOW, 2 * WINDOW), 0)
    cols = lax.broadcasted_iota(jnp.int32, (3 * WINDOW, 2 * WINDOW), 1)
    gap = rows - cols % WINDOW
    near = (gap >= 0) & (gap <= 2 * WINDOW)
    blank = jnp.zeros((HEAD, WINDOW), jnp.bfloat16)
    for n in range(BLK // WINDOW):
        here = slice(n * WINDOW, (n + 1) * WINDOW)
        keys = wkv[n * WINDOW : (n + 3) * WINDOW, :]
        queries = jnp.concatenate(
            [
                jnp.concatenate([wq_ref[0:HEAD, here], blank], axis=0),
                jnp.concatenate([wq_ref[HEAD : 2 * HEAD, here], blank], axis=0),
            ],
            axis=1,
        )
        scores = jnp.dot(keys, queries, preferred_element_type=jnp.float32)
        place = rows + (sp * BLK + (n - 1) * WINDOW)
        allowed = near & (place >= 0) & (place < length_all)
        scores = jnp.where(allowed, scores, -jnp.inf)
        highest = jnp.maximum(jnp.max(scores, axis=0, keepdims=True), sinks)
        weights = jnp.exp2(scores - highest)
        denominators = jnp.sum(weights, axis=0, keepdims=True) + jnp.exp2(sinks - highest)
        mix = jnp.dot(
            values_t[:, n * WINDOW : (n + 3) * WINDOW],
            weights.astype(jnp.bfloat16),
            preferred_element_type=jnp.float32,
        )
        mix = mix / denominators
        both = jnp.concatenate([mix[:, :WINDOW], mix[:, WINDOW:]], axis=0)
        out_ref[here, 2 * HEAD :] = jnp.transpose(both).astype(jnp.bfloat16)


def at_tp(index):
    return {"tp": index}


def remote(src, dst, send, recv, device):
    return pltpu.make_async_remote_copy(
        src_ref=src, dst_ref=dst, send_sem=send, recv_sem=recv, device_id=device, device_id_type=MESH
    )


def turned(rows, half, cosine, sine):
    first, second = rows[:half], rows[half:]
    return [first * cosine - second * sine, second * cosine + first * sine]


def project(
    gain_ref, lgain_ref, near_ref, far_ref, weights, up, kv, q, wkv, wq, xs, squares, accs, x_send, x_recv, ready, raise_ready, send_kv, send_q, send_w
):
    tp = lax.axis_index("tp")
    x, core = tp // 2, tp % 2
    right = ((x + 1) % X) * 2 + core
    left = ((x + X - 1) % X) * 2 + core
    partner = 2 * x + 1 - core

    def half_of(ref, half):
        return ref.at[pl.ds(half * ROWS, ROWS)]

    mine = [2 * r + core for r in range(X)]

    def to_side(half, rightward):
        slot = mine[1] if rightward else mine[3]
        tag = (2 if rightward else 6) + half
        return remote(
            half_of(xs.at[core], half),
            half_of(xs.at[slot], half),
            x_send.at[tag],
            x_recv.at[tag],
            at_tp(right if rightward else left),
        )

    def onward(rightward):
        half = 0 if rightward else 1
        tag = 4 + half
        return remote(
            half_of(xs.at[mine[1] if rightward else mine[3]], half),
            half_of(xs.at[mine[2]], half),
            x_send.at[tag],
            x_recv.at[tag],
            at_tp(right if rightward else left),
        )

    def over(r, half):
        tag = 8 + 2 * r + half
        slot = xs.at[mine[r]]
        return remote(half_of(slot, half), half_of(slot, half), x_send.at[tag], x_recv.at[tag], at_tp(partner))

    own_over = remote(xs.at[core], xs.at[core], x_send.at[0], x_recv.at[0], at_tp(partner))
    to_side(0, True).start()
    to_side(1, False).start()
    own_over.start()
    to_side(1, True).start()
    to_side(0, False).start()
    ready()

    def add(r):
        chip = (x + (0, X - 1, 2, 1)[r]) % X
        values = jnp.concatenate([xs[2 * r], xs[2 * r + 1]], axis=1).astype(jnp.float32)
        square = values * values
        square = square[:, 0:128] + square[:, 128:256] + square[:, 256:384] + square[:, 384:512]
        rows = pl.ds(pl.multiple_of(chip * 2 * COLS, 2 * COLS), 2 * COLS)
        scaled = (values * gain_ref[:, rows]).astype(jnp.bfloat16)
        if r == 0:
            squares[...] = square
        else:
            squares[...] += square
        slim = lax.dot_general(
            weights[0][:, rows], scaled, (((1,), (1,)), ((), ())), preferred_element_type=jnp.float32
        )
        products = [slim] + [
            jnp.dot(scaled, weight[rows, :], preferred_element_type=jnp.float32) for weight in weights[1:]
        ]
        for product, acc in zip(products, accs):
            if r == 0:
                acc[...] = product
            else:
                acc[...] += product

    own_over.wait_recv()
    add(0)
    to_side(0, True).wait_recv()
    onward(True).start()
    over(1, 0).start()
    to_side(1, False).wait_recv()
    onward(False).start()
    over(3, 1).start()
    to_side(1, True).wait_recv()
    over(1, 1).start()
    to_side(0, False).wait_recv()
    over(3, 0).start()
    for half in range(2):
        over(1, half).wait_recv()
    add(1)
    for half in range(2):
        over(3, half).wait_recv()
    add(3)
    onward(True).wait_recv()
    over(2, 0).start()
    onward(False).wait_recv()
    over(2, 1).start()
    for half in range(2):
        over(2, half).wait_recv()
    add(2)

    width = 2 * COLS * X
    scale = lax.rsqrt(jnp.sum(squares[...], axis=1, keepdims=True) / width + epsilon)
    acc_slim, acc_ld, acc_wq = accs
    row_scale = lax.rsqrt(jnp.sum(jnp.transpose(squares[...]), axis=0, keepdims=True) / width + epsilon)
    turn = far_ref[...]
    here = lax.broadcasted_iota(jnp.int32, turn.shape, 2) == lax.axis_index("sp")
    turn = jnp.sum(jnp.where(here, turn, 0.0), axis=2, keepdims=True)
    far_cos, far_sin = turn[0], turn[1]
    near_cos, near_sin = near_ref[0], near_ref[1]
    cosine = far_cos * near_cos - far_sin * near_sin
    sine = far_sin * near_cos + far_cos * near_sin
    wide_cos, wide_sin = cosine[0:32], sine[0:32]
    slim_cos, slim_sin = cosine[32:48], sine[32:48]
    mixed = acc_slim[0 : SLIM[2]] * row_scale
    keys = jnp.concatenate(turned(mixed[SLIM[0] : SLIM[1]], HEAD // 2, wide_cos, wide_sin), axis=0)
    values_t = mixed[SLIM[1] : SLIM[2]]
    wkv[...] = jnp.transpose(jnp.concatenate([keys, values_t], axis=0)).astype(jnp.bfloat16)
    send_w()
    sharp = LOG2E * (NOPE + ROPE) ** (-0.5)
    wide = NOPE + ROPE
    pieces = [mixed[0:NOPE], mixed[wide : wide + NOPE]]
    for h in range(2):
        pieces += turned(mixed[wide * h + NOPE : wide * (h + 1)], ROPE // 2, slim_cos, slim_sin)
    q[...] = (jnp.concatenate(pieces, axis=0) * sharp).astype(jnp.bfloat16)
    send_q()
    raise_ready()
    low = acc_ld[...] * scale
    low = low * lax.rsqrt(jnp.mean(low * low, axis=1, keepdims=True) + epsilon) * lgain_ref[0:1, :]
    expanded = jnp.dot(low.astype(jnp.bfloat16), up[...], preferred_element_type=jnp.float32)
    lane = lax.broadcasted_iota(jnp.int32, (BLK, 128), 1)
    one, two = expanded[:, 0:128], expanded[:, 128:256]
    kv[0:BLK, :] = jnp.where(lane < HEAD, one, pltpu.roll(two, HEAD, 1)).astype(jnp.bfloat16)
    values = jnp.where(lane < HEAD, pltpu.roll(one, HEAD, 1), two)
    for k in range(4):
        block = slice(BLK + 128 * k, BLK + 128 * (k + 1))
        kv[block, :] = jnp.transpose(values[128 * k : 128 * (k + 1)]).astype(jnp.bfloat16)
    shared = acc_slim[SLIM[2] : SLIM[3]] * row_scale
    shared = jnp.concatenate(turned(shared, ROPE // 2, slim_cos, slim_sin), axis=0)
    packed = jnp.concatenate([shared[:, 128 * k : 128 * (k + 1)] for k in range(4)], axis=0)
    kv[2 * BLK :, :] = jnp.transpose(packed).astype(jnp.bfloat16)
    send_kv()
    queries = jnp.transpose(acc_wq[...] * scale)
    pieces = []
    for h in range(2):
        pieces += turned(queries[HEAD * h : HEAD * (h + 1)], HEAD // 2, wide_cos, wide_sin)
    wq[...] = (jnp.concatenate(pieces, axis=0) * (LOG2E * HEAD ** (-0.5))).astype(jnp.bfloat16)

    sent = [own_over, onward(True), onward(False)]
    sent += [to_side(half, way) for half in range(2) for way in (True, False)]
    sent += [over(r, half) for r in (1, 2, 3) for half in range(2)]
    return sent


def reduce(mixed, wl, ww, out_ref, pair_out, pair_in, passed, gone, kept, side_out, side_in, r_send, r_recv):
    tp = lax.axis_index("tp")
    x, core = tp // 2, tp % 2
    right = ((x + 1) % X) * 2 + core
    left = ((x + X - 1) % X) * 2 + core
    partner = 2 * x + 1 - core
    values = mixed[...]

    def projected(r, core_to):
        block = ((x + r) % X) * 2 + core_to
        cols = pl.ds(pl.multiple_of(block * COLS, COLS), COLS)
        weight = jnp.concatenate([wl[:, cols], ww[:, cols]], axis=0)
        return jnp.dot(values, weight, preferred_element_type=jnp.float32)

    def pair(r):
        return remote(pair_out.at[r], pair_in.at[r], r_send.at[r], r_recv.at[r], at_tp(partner))

    def far(half):
        return remote(
            gone.at[half], passed.at[half], r_send.at[4 + half], r_recv.at[4 + half], at_tp((right, left)[half])
        )

    def side(rightward, half):
        tag = 2 * (0 if rightward else 1) + half
        return remote(
            side_out.at[tag], side_in.at[tag], r_send.at[6 + tag], r_recv.at[6 + tag], at_tp(right if rightward else left)
        )

    def start_pair(r):
        pair_out[r] = projected(r, 1 - core).astype(jnp.bfloat16)
        pair(r).start()

    order = (2, 1, 3, 0)
    start_pair(2)
    own_next = projected(2, core)
    start_pair(1)
    for n, r in enumerate(order):
        own = own_next
        pair(r).wait_recv()
        total = own + pair_in[r].astype(jnp.float32)
        upper, lower = total[:ROWS], total[ROWS:]
        if r == 2:
            gone[0] = upper.astype(jnp.bfloat16)
            far(0).start()
            gone[1] = lower.astype(jnp.bfloat16)
            far(1).start()
        elif r == 1:
            side_out[1] = lower.astype(jnp.bfloat16)
            side(True, 1).start()
            kept[0] = upper
        elif r == 3:
            side_out[2] = upper.astype(jnp.bfloat16)
            side(False, 0).start()
            kept[1] = lower
        else:
            kept[2] = upper
            kept[3] = lower
        if n < 2:
            start_pair(order[n + 2])
        if n < 3:
            own_next = projected(order[n + 1], core)
    far(0).wait_recv()
    side_out[0] = (kept[0] + passed[0].astype(jnp.float32)).astype(jnp.bfloat16)
    side(True, 0).start()
    far(1).wait_recv()
    side_out[3] = (kept[1] + passed[1].astype(jnp.float32)).astype(jnp.bfloat16)
    side(False, 1).start()
    for half in (1, 0):
        side(True, half).wait_recv()
        side(False, half).wait_recv()
    for half in range(2):
        total = kept[2 + half] + side_in[half].astype(jnp.float32) + side_in[2 + half].astype(jnp.float32)
        out_ref[half * ROWS : (half + 1) * ROWS, :] = total.astype(jnp.bfloat16)
    sent = [pair(r) for r in range(X)] + [far(half) for half in range(2)]
    return sent + [side(way, half) for way in (True, False) for half in range(2)]


SLIM = (192, 256, 320, 352)


def layer_kernel(
    length_all,
    sink_ref,
    x_hbm,
    gain_hbm,
    lgain_hbm,
    near_hbm,
    far_hbm,
    lq_hbm,
    wk_hbm,
    wv_hbm,
    rd_hbm,
    ld_hbm,
    wq_hbm,
    up_hbm,
    ol_hbm,
    ow_hbm,
    result_ref,
    gain_ref,
    lgain_ref,
    near_ref,
    far_ref,
    w_slim,
    w_ld,
    w_wq,
    w_up,
    w_ol,
    w_ow,
    xs,
    squares,
    a_slim,
    a_ld,
    a_wq,
    kv_ref,
    q_ref,
    wkv_ref,
    wq_ref,
    out_ref,
    kvs,
    ropes,
    qraw,
    qpad,
    wkv,
    s0,
    s1,
    now_max,
    now_shrink,
    run_max,
    acc,
    o_out,
    o_in,
    pair_out,
    pair_in,
    passed,
    gone,
    kept,
    side_out,
    side_in,
    load_sem,
    x_send,
    x_recv,
    kv_send,
    kv_recv,
    q_send,
    q_recv,
    o_send,
    o_recv,
    w_send,
    w_recv,
    r_send,
    r_recv,
):
    sp = lax.axis_index("sp")
    z, y = sp // Y, sp % Y
    up = ((z + 1) % Z) * Y + y
    down = ((z + Z - 1) % Z) * Y + y
    right = z * Y + (y + 1) % Y
    left = z * Y + (y + Y - 1) % Y
    across = z * Y + (y + 2) % Y
    after = (sp + 1) % (Z * Y)
    before = (sp + Z * Y - 1) % (Z * Y)
    barrier = pltpu.get_barrier_semaphore()
    peers = [at_sp(peer) for peer in (up, down, right, left, across, after, before)]
    tp = lax.axis_index("tp")
    x, core = tp // 2, tp % 2
    peers += [at_tp((tp + 2) % (2 * X)), at_tp((tp + 2 * X - 2) % (2 * X)), at_tp(2 * x + 1 - core)]
    for peer in peers:
        pl.semaphore_signal(barrier, inc=1, device_id=peer, device_id_type=MESH)
    load_x = pltpu.make_async_copy(x_hbm, xs.at[core], load_sem.at[13])
    load_x.start()
    sources = (gain_hbm, lgain_hbm, near_hbm, far_hbm, lq_hbm, wk_hbm, wv_hbm, rd_hbm, ld_hbm, wq_hbm, up_hbm, ol_hbm, ow_hbm)
    ends = (0, *SLIM)
    targets = [gain_ref, lgain_ref, near_ref, far_ref]
    targets += [w_slim.at[pl.ds(a, b - a)] for a, b in zip(ends, SLIM)] + [w_ld, w_wq, w_up, w_ol, w_ow]
    loads = [
        pltpu.make_async_copy(source, target, load_sem.at[n])
        for n, (source, target) in enumerate(zip(sources, targets))
    ]
    for load in loads:
        load.start()
    load_x.wait()
    pl.semaphore_wait(barrier, len(peers))

    def copy(src, dst, send, recv, peer):
        return pltpu.make_async_remote_copy(
            src_ref=src,
            dst_ref=dst,
            send_sem=send,
            recv_sem=recv,
            device_id=at_sp(peer),
            device_id_type=MESH,
        )

    def kv_half(ref, half):
        return ref.at[pl.ds(half * HALF, HALF)]

    def kv_copy(step, half, upward):
        came = 0 if step == 1 else (2 * step - 3 if upward else 2 * step - 2)
        goes = 7 if step == 4 else (2 * step - 1 if upward else 2 * step)
        src = kv_half(kv_ref if step == 1 else kvs.at[came], half)
        slot = 2 * goes + half
        return copy(
            src, kv_half(kvs.at[goes], half), kv_send.at[slot], kv_recv.at[slot], up if upward else down
        )

    q_half = q_ref.shape[0] // 2
    q_right = copy(q_ref, qraw.at[1], q_send.at[0], q_recv.at[0], right)
    q_left = copy(q_ref, qraw.at[2], q_send.at[1], q_recv.at[1], left)
    q_on_right = copy(
        qraw.at[1, pl.ds(0, q_half)], qraw.at[3, pl.ds(0, q_half)], q_send.at[2], q_recv.at[2], right
    )
    q_on_left = copy(
        qraw.at[2, pl.ds(q_half, q_half)], qraw.at[3, pl.ds(q_half, q_half)], q_send.at[3], q_recv.at[3], left
    )
    w_after = copy(
        wkv_ref.at[pl.ds(BLK - WINDOW, WINDOW)], wkv.at[pl.ds(0, WINDOW)], w_send.at[0], w_recv.at[0], after
    )
    w_before = copy(
        wkv_ref.at[pl.ds(0, WINDOW)], wkv.at[pl.ds(BLK + WINDOW, WINDOW)], w_send.at[1], w_recv.at[1], before
    )

    def load_weights():
        run_max[...] = jnp.full(run_max.shape, -1e30, jnp.float32)
        acc[...] = jnp.zeros(acc.shape, jnp.float32)
        for load in loads[:-3]:
            load.wait()

    def send_kv():
        for load in loads[-2:]:
            load.wait()
        for half in range(2):
            kv_copy(1, half, True).start()
            kv_copy(1, half, False).start()

    def send_q():
        q_right.start()
        q_left.start()

    def send_w():
        w_after.start()
        w_before.start()

    x_sent = project(
        gain_ref,
        lgain_ref,
        near_ref,
        far_ref,
        (w_slim, w_ld, w_wq),
        w_up,
        kv_ref,
        q_ref,
        wkv_ref,
        wq_ref,
        xs,
        squares,
        (a_slim, a_ld, a_wq),
        x_send,
        x_recv,
        load_weights,
        loads[-3].wait,
        send_kv,
        send_q,
        send_w,
    )

    scores_of = (s0, s1)
    blank = jnp.zeros((NOPE, BLK), jnp.bfloat16)

    def set_queries(g, src):
        qpad[2 * g, 0:NOPE] = src[0:NOPE, :]
        qpad[2 * g, NOPE : 2 * NOPE] = blank
        qpad[2 * g + 1, 0:NOPE] = blank
        qpad[2 * g + 1, NOPE : 2 * NOPE] = src[NOPE : 2 * NOPE, :]
        for h in range(2):
            start = 2 * NOPE + h * ROPE
            qpad[2 * g + h, 2 * NOPE : 2 * NOPE + ROPE] = src[start : start + ROPE, :]
            qpad[2 * g + h, 2 * NOPE + ROPE :] = jnp.zeros((128 - ROPE, BLK), jnp.bfloat16)

    def set_ropes(p, packed):
        wide = packed.astype(jnp.float32)
        ropes[p, 0:128] = packed
        for k in range(1, 4):
            ropes[p, 128 * k : 128 * (k + 1)] = pltpu.roll(wide, 128 - 32 * k, 1).astype(jnp.bfloat16)

    def keys_of(p):
        return jnp.concatenate([kvs[p, 0:BLK, :], ropes[p]], axis=1)

    def scores_stage(p, g, h):
        scores = jnp.dot(keys_of(p), qpad[2 * g + h], preferred_element_type=jnp.float32)
        scores_of[h][...] = scores
        before_max = run_max[2 * g + h]
        highest = jnp.maximum(before_max, jnp.max(scores, axis=0, keepdims=True))
        now_shrink[h] = jnp.exp2(before_max - highest)
        now_max[h] = highest
        run_max[2 * g + h] = highest

    def values_stage(p, g, h):
        weights = jnp.exp2(scores_of[h][...] - now_max[h]).astype(jnp.bfloat16)
        values = jnp.concatenate(
            [kvs[p, pl.ds(BLK + 128 * k + HEAD * h, HEAD), :] for k in range(4)], axis=1
        )
        values = jnp.concatenate([values, jnp.ones((16, BLK), jnp.bfloat16)], axis=0)
        mix = jnp.dot(values, weights, preferred_element_type=jnp.float32)
        acc[2 * g + h] = acc[2 * g + h] * now_shrink[h] + mix

    def finish(g, h):
        total = acc[2 * g + h]
        denominator = total[HEAD : HEAD + 1]
        return total[:HEAD] / denominator, run_max[2 * g + h] + jnp.log2(denominator)

    def o_copy(g):
        peer = (None, left, right, across)[g]
        return copy(o_out.at[g - 1], o_in.at[g - 1], o_send.at[g - 1], o_recv.at[g - 1], peer)

    def send_out(g):
        tails = []
        for h in range(2):
            out, level = finish(g, h)
            o_out[g - 1, HEAD * h : HEAD * (h + 1)] = out.astype(jnp.bfloat16)
            tails += [part.astype(jnp.float32) for part in split3(level)]
        tails.append(jnp.zeros((10, BLK), jnp.float32))
        o_out[g - 1, 2 * HEAD :] = jnp.concatenate(tails, axis=0).astype(jnp.bfloat16)
        o_copy(g).start()

    def unit(u):
        p, g = jnp.where(u < 3, 0, 1 + (u - 3) // 2), jnp.where(u < 3, u, 1 + (u - 3) % 2)
        p, g = jnp.where(u < 7, p, u - 7), jnp.where(u < 7, g, 3)
        p, g = jnp.where(u < 10, p, 3 + (u - 10) // 4), jnp.where(u < 10, g, (u - 10) % 4)
        p, g = jnp.where(u < 18, p, 5 + (u - 18) // 3), jnp.where(u < 18, g, 3 - (u - 18) % 3)
        p = jnp.where(u < 27, p, jnp.where(u < 29, u - 26, u - 24))
        g = jnp.where(u < 27, g, 0)
        return p, g

    kvs[0] = kv_ref[...]
    set_queries(0, q_ref)
    set_ropes(0, kv_ref[2 * BLK :, :])
    wkv[WINDOW : WINDOW + BLK, :] = wkv_ref[...]
    w_after.wait_recv()
    w_before.wait_recv()
    window_part(wkv, wq_ref, sink_ref, out_ref, sp, length_all)
    scores_stage(0, 0, 0)

    def arrive(step, half):
        kv_copy(step, half, True).wait_recv()
        kv_copy(step, half, False).wait_recv()

    def at0():
        q_right.wait_recv()
        q_on_right.start()
        q_left.wait_recv()
        q_on_left.start()
        set_queries(1, qraw.at[1])
        set_queries(2, qraw.at[2])

    def at1():
        arrive(1, 0)
        kv_copy(2, 0, True).start()
        kv_copy(2, 0, False).start()

    def at2():
        arrive(1, 1)
        kv_copy(2, 1, True).start()
        kv_copy(2, 1, False).start()
        set_ropes(1, kvs[1, 2 * BLK :, :])
        set_ropes(2, kvs[2, 2 * BLK :, :])

    def at5():
        arrive(2, 0)
        kv_copy(3, 0, True).start()
        kv_copy(3, 0, False).start()

    def at6():
        q_on_right.wait_recv()
        q_on_left.wait_recv()
        set_queries(3, qraw.at[3])

    def at9():
        arrive(2, 1)
        kv_copy(3, 1, True).start()
        kv_copy(3, 1, False).start()
        set_ropes(3, kvs[3, 2 * BLK :, :])
        set_ropes(4, kvs[4, 2 * BLK :, :])

    def at13():
        arrive(3, 0)
        kv_copy(4, 0, True).start()

    def at17():
        arrive(3, 1)
        kv_copy(4, 1, False).start()
        set_ropes(5, kvs[5, 2 * BLK :, :])
        set_ropes(6, kvs[6, 2 * BLK :, :])

    def at23():
        kv_copy(4, 0, True).wait_recv()
        kv_copy(4, 1, False).wait_recv()
        set_ropes(7, kvs[7, 2 * BLK :, :])

    events = {
        0: at0,
        1: at1,
        2: at2,
        5: at5,
        6: at6,
        9: at9,
        13: at13,
        17: at17,
        23: at23,
        25: lambda: send_out(3),
        26: lambda: send_out(2),
        27: lambda: send_out(1),
    }

    def advance(u, carry):
        for when, event in events.items():
            pl.when(u == when)(event)
        p, g = unit(u)
        p_next, g_next = unit(jnp.minimum(u + 1, 31))
        scores_stage(p, g, 1)
        values_stage(p, g, 0)
        scores_stage(p_next, g_next, 0)
        values_stage(p, g, 1)
        return carry

    lax.fori_loop(0, 32, advance, 0)

    own = [finish(0, h) for h in range(2)]
    for g in range(1, 4):
        o_copy(g).wait_recv()
    merged = []
    for h in range(2):
        outs, levels = [own[h][0]], [own[h][1]]
        for g in range(1, 4):
            block = o_in[g - 1].astype(jnp.float32)
            outs.append(block[HEAD * h : HEAD * (h + 1)])
            row = 2 * HEAD + 3 * h
            levels.append(block[row : row + 1] + block[row + 1 : row + 2] + block[row + 2 : row + 3])
        top = functools.reduce(jnp.maximum, levels)
        shares = [jnp.exp2(level - top) for level in levels]
        total = functools.reduce(jnp.add, shares)
        mixed = functools.reduce(jnp.add, [o * (s / total) for o, s in zip(outs, shares)])
        merged.append(mixed)
    out_ref[:, 0 : 2 * HEAD] = jnp.transpose(jnp.concatenate(merged, axis=0)).astype(jnp.bfloat16)

    r_sent = reduce(
        out_ref, w_ol, w_ow, result_ref, pair_out, pair_in, passed, gone, kept, side_out, side_in, r_send, r_recv
    )

    w_sends = [w_after, w_before, q_right, q_left, q_on_right, q_on_left]
    for step in range(1, 4):
        for half in range(2):
            w_sends += [kv_copy(step, half, True), kv_copy(step, half, False)]
    w_sends += [kv_copy(4, 0, True), kv_copy(4, 1, False)]
    w_sends += [o_copy(g) for g in range(1, 4)]
    for sent in w_sends + x_sent + r_sent:
        sent.wait_send()


def tables():
    near, freqs = [], []
    for width in (HEAD, ROPE):
        half = width // 2
        freqs.append(10000.0 ** (-np.arange(half) / half))
    freqs = np.concatenate(freqs)
    angles = freqs[:, None] * np.arange(BLK)[None, :]
    near = np.stack([np.cos(angles), np.sin(angles)]).astype(np.float32)
    angles = freqs[:, None] * (BLK * np.arange(128))[None, :]
    far = np.stack([np.cos(angles), np.sin(angles)]).astype(np.float32)
    return near, far


def shards(
    inputs,
    norm_gain,
    latent_query,
    latent_down,
    rope_down,
    latent_gain,
    latent_up,
    window_query,
    window_key,
    window_value,
    sink_logit,
    out_latent,
    out_window,
):
    length_all = BLK * Z * Y
    near, far = tables()
    dma = pltpu.SemaphoreType.DMA
    bf16, f32 = jnp.bfloat16, jnp.float32
    in_vmem = pl.BlockSpec(memory_space=pltpu.VMEM)
    in_smem = pl.BlockSpec(memory_space=pltpu.SMEM)
    in_hbm = pl.BlockSpec(memory_space=pltpu.HBM)
    rows = norm_gain.shape[0]
    return pl.pallas_call(
        functools.partial(layer_kernel, length_all),
        out_shape=jax.ShapeDtypeStruct((BLK, COLS), bf16),
        in_specs=[in_smem] + [in_hbm] * 14,
        out_specs=in_vmem,
        scratch_shapes=[
            pltpu.VMEM((1, rows), f32),
            pltpu.VMEM((1, latent_gain.shape[0]), f32),
            pltpu.VMEM(near.shape, f32),
            pltpu.VMEM(far.shape, f32),
            pltpu.VMEM((SLIM[3], rows), bf16),
            pltpu.VMEM(latent_down.shape, bf16),
            pltpu.VMEM(window_query.shape, bf16),
            pltpu.VMEM(latent_up.shape, bf16),
            pltpu.VMEM(out_latent.shape, bf16),
            pltpu.VMEM(out_window.shape, bf16),
            pltpu.VMEM((2 * X, BLK, COLS), bf16),
            pltpu.VMEM((BLK, 128), f32),
            pltpu.VMEM((SLIM[3], BLK), f32),
            pltpu.VMEM((BLK, latent_down.shape[1]), f32),
            pltpu.VMEM((BLK, window_query.shape[1]), f32),
            pltpu.VMEM((KV_ROWS, 128), bf16),
            pltpu.VMEM((2 * (NOPE + ROPE), BLK), bf16),
            pltpu.VMEM((BLK, 2 * HEAD), bf16),
            pltpu.VMEM((2 * HEAD, BLK), bf16),
            pltpu.VMEM((BLK, 4 * HEAD), bf16),
            pltpu.VMEM((Z, KV_ROWS, 128), bf16),
            pltpu.VMEM((Z, BLK, 128), bf16),
            pltpu.VMEM((Y, 2 * (NOPE + ROPE), BLK), bf16),
            pltpu.VMEM((2 * Y, 256, BLK), bf16),
            pltpu.VMEM((BLK + 2 * WINDOW, 128), bf16),
            pltpu.VMEM((BLK, BLK), f32),
            pltpu.VMEM((BLK, BLK), f32),
            pltpu.VMEM((2, 1, BLK), f32),
            pltpu.VMEM((2, 1, BLK), f32),
            pltpu.VMEM((2 * Y, 1, BLK), f32),
            pltpu.VMEM((2 * Y, HEAD + 16, BLK), f32),
            pltpu.VMEM((Y - 1, O_ROWS, BLK), bf16),
            pltpu.VMEM((Y - 1, O_ROWS, BLK), bf16),
            pltpu.VMEM((X, BLK, COLS), bf16),
            pltpu.VMEM((X, BLK, COLS), bf16),
            pltpu.VMEM((2, ROWS, COLS), bf16),
            pltpu.VMEM((2, ROWS, COLS), bf16),
            pltpu.VMEM((4, ROWS, COLS), f32),
            pltpu.VMEM((4, ROWS, COLS), bf16),
            pltpu.VMEM((4, ROWS, COLS), bf16),
            dma((14,)),
            dma((16,)),
            dma((16,)),
            dma((16,)),
            dma((16,)),
            dma((4,)),
            dma((4,)),
            dma((3,)),
            dma((3,)),
            dma((2,)),
            dma((2,)),
            dma((10,)),
            dma((10,)),
        ],
        compiler_params=pltpu.CompilerParams(
            collective_id=1, has_side_effects=True, vmem_limit_bytes=VMEM_LIMIT
        ),
        name="layer",
    )(
        sink_logit,
        inputs,
        norm_gain[None, :],
        latent_gain[None, :],
        near,
        far,
        latent_query.T,
        window_key.T,
        window_value.T,
        rope_down.T,
        latent_down,
        window_query,
        latent_up,
        out_latent,
        out_window,
    )


def solution(mesh):
    in_specs = (
        P("sp", "tp"),
        P(),
        P(None, "tp"),
        P(),
        P(),
        P(),
        P(None, "tp"),
        P(None, "tp"),
        P(None, "tp"),
        P(None, "tp"),
        P("tp"),
        P("tp", None),
        P("tp", None),
    )
    out_specs = P("sp", "tp")
    return jax.shard_map(shards, mesh=mesh, in_specs=in_specs, out_specs=out_specs, check_vma=False)
```

time: 145 us -> 77 us (0.53)
  blocking collectives: 32.3 us -> 0 us
  Pallas kernels: 43.8 us -> 75.2 us
  waiting for transfers between devices: 22.7 us -> 0 us
  other arithmetic: 13.8 us -> 0 us
  local copies, waits for them, and re-layouts: 13.6 us -> 1.67 us
  matrix products: 10.7 us -> 0 us
  starting transfers between devices: 7.56 us -> 0 us
    all_to_all x1 -> x0, blocking collectives: 32.3 us -> none  [summed_on_arrival(): lax.all_to_all(parts, axis, split_axis=0, concat_axis=0, tiled=True)]
    pallas_call x1, Pallas kernels: 43.8 us -> 75.2 us  [shards(): pl.pallas_call(functools.partial(layer_kernel, length_all), out_shape=jax...]
    all_to_all x1 -> x0, waiting for transfers between devices: 22.7 us -> none  [sent_to_all(): lax.all_to_all(jnp.broadcast_to(value[None], (peers, *value.shape)), axis...]
    dot_general x9 -> x0, matrix products: 10.7 us -> none  [the longest x1 2.91 us: shards(): jnp.dot(hidden, latent_down, preferred_element_type=jnp.float32)]
    all_to_all x1 -> x0, starting transfers between devices: 7.56 us -> none  [sent_to_all(): lax.all_to_all(jnp.broadcast_to(value[None], (peers, *value.shape)), axis...]
    reduce_sum x2 -> x0, other arithmetic: 4.22 us -> none  [the longest x1 2.25 us: rms_scale(): jnp.mean(values * values, axis=-1, keepdims=True) + epsilon]
    all_to_all x1 -> x0, local copies, waits for them, and re-layouts: 3.91 us -> none  [sent_to_all(): lax.all_to_all(jnp.broadcast_to(value[None], (peers, *value.shape)), axis...]
    broadcast_in_dim x2 -> x0, local copies, waits for them, and re-layouts: 3.18 us -> none  [the longest x1 2.53 us: sent_to_all(): jnp.broadcast_to(value[None], (peers, *value.shape))]
  transfers between devices with their start and end apart: 1 -> 0, of which waited for: 1 -> 0; matrix products, arithmetic and copies ran while one was open for 2% -> 0% of each run, Pallas kernels for 0% -> 0%
where the time goes in v2:
time: 77 us; the launch traced here: 76.8 us
  Pallas kernels  75.2 us (98%)
  local copies, waits for them, and re-layouts  1.67 us (2%)
    pallas_call x1, Pallas kernels, shards(): pl.pallas_call(functools.partial(layer_kernel, length_all), out_shape=jax...  75.2 us
    unnamed x1, local copies, waits for them, and re-layouts  1.67 us

profile of v2, /device:TPU:1, one launch (start us, length us, event | category | flops | bytes accessed | tf_op | source)
XLA Modules:
  0.0 76.8 jit_solution(13737684712250498795)
XLA Ops:
  0.0 75.2 %layer.1 = bf16[512,256]{1,0:T(8,128)(2,1)} custom-call(f32[2]{0:T(128)} %sink_ref.1, bf16[512,256]{1,0:T(8,128)(2,1)} %x_hbm.1, f32[1,2048]{1,0:T(1,128)} %bitcast.10, f32[1,512]{1,0:T(1,128)} %bitcast.11, f32[2,48,512]{2,1,0:T(8,128)} %constant.4.clone.near_hbm, f32[2,48,128]{2,1,0:T(8,128)} %constant.5.clone.far_hbm, bf16[192,2048]{1,0:T(8,128)(2,1)} %bitcast.6, ...), custom_call_target="tpu_custom_call" | custom-call | tf_op jit(solution)/shard_map/layer/pallas_call | solution.py:739
  75.2 1.7 %copy.17 = bf16[512,256]{1,0:T(8,128)(2,1)} copy(bf16[512,256]{1,0:T(8,128)(2,1)} %layer.1) | data formatting | bytes 524288

commit v3 on v2

--- a/solution.py
+++ b/solution.py
@@ -18,11 +18,13 @@
 VMEM_LIMIT = 60 * 2**20
 Z, Y, X = 8, 4, 4
 BLK = 512
-KV_ROWS = BLK + BLK + BLK // 4
-HALF = KV_ROWS // 2
+HALF = BLK // 2 + BLK // 2 + BLK // 8
 O_ROWS = 2 * HEAD + 16
 COLS = 256
 ROWS = BLK // 2
+QUARTER = BLK // 4
+TILE = 256
+PAIRS = Y * Z // 2
 
 
 epsilon = 1e-06
@@ -100,99 +102,70 @@
     left = ((x + X - 1) % X) * 2 + core
     partner = 2 * x + 1 - core
 
-    def half_of(ref, half):
-        return ref.at[pl.ds(half * ROWS, ROWS)]
+    def rows_of(ref, start, size):
+        return ref.at[pl.ds(start, size)]
 
     mine = [2 * r + core for r in range(X)]
 
-    def to_side(half, rightward):
+    def to_side(quarter, rightward):
         slot = mine[1] if rightward else mine[3]
-        tag = (2 if rightward else 6) + half
+        tag = quarter + (0 if rightward else 4)
         return remote(
-            half_of(xs.at[core], half),
-            half_of(xs.at[slot], half),
+            rows_of(xs.at[core], quarter * QUARTER, QUARTER),
+            rows_of(xs.at[slot], quarter * QUARTER, QUARTER),
             x_send.at[tag],
             x_recv.at[tag],
             at_tp(right if rightward else left),
         )
 
-    def onward(rightward):
-        half = 0 if rightward else 1
-        tag = 4 + half
+    def onward(half, rightward):
+        start = half * ROWS + (0 if rightward else QUARTER)
+        tag = 8 + 2 * half + (0 if rightward else 1)
         return remote(
-            half_of(xs.at[mine[1] if rightward else mine[3]], half),
-            half_of(xs.at[mine[2]], half),
+            rows_of(xs.at[mine[1] if rightward else mine[3]], start, QUARTER),
+            rows_of(xs.at[mine[2]], start, QUARTER),
             x_send.at[tag],
             x_recv.at[tag],
             at_tp(right if rightward else left),
         )
 
     def over(r, half):
-        tag = 8 + 2 * r + half
-        slot = xs.at[mine[r]]
-        return remote(half_of(slot, half), half_of(slot, half), x_send.at[tag], x_recv.at[tag], at_tp(partner))
-
-    own_over = remote(xs.at[core], xs.at[core], x_send.at[0], x_recv.at[0], at_tp(partner))
-    to_side(0, True).start()
-    to_side(1, False).start()
-    own_over.start()
-    to_side(1, True).start()
-    to_side(0, False).start()
+        tag = 12 + 2 * r + half
+        slot = rows_of(xs.at[mine[r]], half * ROWS, ROWS)
+        return remote(slot, slot, x_send.at[tag], x_recv.at[tag], at_tp(partner))
+
+    for quarter in (0, 1, 2):
+        to_side(quarter, True).start()
+        to_side((1, 0, 3)[quarter], False).start()
+    over(0, 0).start()
+    over(0, 1).start()
     ready()
 
-    def add(r):
+    def add(r, half):
         chip = (x + (0, X - 1, 2, 1)[r]) % X
-        values = jnp.concatenate([xs[2 * r], xs[2 * r + 1]], axis=1).astype(jnp.float32)
+        here = slice(half * ROWS, (half + 1) * ROWS)
+        values = jnp.concatenate([xs[2 * r, here], xs[2 * r + 1, here]], axis=1).astype(jnp.float32)
         square = values * values
         square = square[:, 0:128] + square[:, 128:256] + square[:, 256:384] + square[:, 384:512]
         rows = pl.ds(pl.multiple_of(chip * 2 * COLS, 2 * COLS), 2 * COLS)
         scaled = (values * gain_ref[:, rows]).astype(jnp.bfloat16)
-        if r == 0:
-            squares[...] = square
-        else:
-            squares[...] += square
         slim = lax.dot_general(
             weights[0][:, rows], scaled, (((1,), (1,)), ((), ())), preferred_element_type=jnp.float32
         )
-        products = [slim] + [
-            jnp.dot(scaled, weight[rows, :], preferred_element_type=jnp.float32) for weight in weights[1:]
-        ]
-        for product, acc in zip(products, accs):
-            if r == 0:
-                acc[...] = product
-            else:
-                acc[...] += product
-
-    own_over.wait_recv()
-    add(0)
-    to_side(0, True).wait_recv()
-    onward(True).start()
-    over(1, 0).start()
-    to_side(1, False).wait_recv()
-    onward(False).start()
-    over(3, 1).start()
-    to_side(1, True).wait_recv()
-    over(1, 1).start()
-    to_side(0, False).wait_recv()
-    over(3, 0).start()
-    for half in range(2):
-        over(1, half).wait_recv()
-    add(1)
-    for half in range(2):
-        over(3, half).wait_recv()
-    add(3)
-    onward(True).wait_recv()
-    over(2, 0).start()
-    onward(False).wait_recv()
-    over(2, 1).start()
-    for half in range(2):
-        over(2, half).wait_recv()
-    add(2)
+        wide = [jnp.dot(scaled, weight[rows, :], preferred_element_type=jnp.float32) for weight in weights[1:]]
+        if r == 0:
+            squares[here, :] = square
+            accs[0][:, here] = slim
+            for product, acc in zip(wide, accs[1:]):
+                acc[here, :] = product
+        else:
+            squares[here, :] += square
+            accs[0][:, here] += slim
+            for product, acc in zip(wide, accs[1:]):
+                acc[here, :] += product
 
     width = 2 * COLS * X
-    scale = lax.rsqrt(jnp.sum(squares[...], axis=1, keepdims=True) / width + epsilon)
     acc_slim, acc_ld, acc_wq = accs
-    row_scale = lax.rsqrt(jnp.sum(jnp.transpose(squares[...]), axis=0, keepdims=True) / width + epsilon)
     turn = far_ref[...]
     here = lax.broadcasted_iota(jnp.int32, turn.shape, 2) == lax.axis_index("sp")
     turn = jnp.sum(jnp.where(here, turn, 0.0), axis=2, keepdims=True)
@@ -202,43 +175,106 @@
     sine = far_sin * near_cos + far_cos * near_sin
     wide_cos, wide_sin = cosine[0:32], sine[0:32]
     slim_cos, slim_sin = cosine[32:48], sine[32:48]
+
+    def make_kv(half):
+        here = slice(half * ROWS, (half + 1) * ROWS)
+        square = squares[here, :]
+        scale = lax.rsqrt(jnp.sum(square, axis=1, keepdims=True) / width + epsilon)
+        low = acc_ld[here, :] * scale
+        low = low * lax.rsqrt(jnp.mean(low * low, axis=1, keepdims=True) + epsilon) * lgain_ref[0:1, :]
+        expanded = jnp.dot(low.astype(jnp.bfloat16), up[...], preferred_element_type=jnp.float32)
+        lane = lax.broadcasted_iota(jnp.int32, (ROWS, 128), 1)
+        one, two = expanded[:, 0:128], expanded[:, 128:256]
+        kv[half, 0:ROWS, :] = jnp.where(lane < HEAD, one, pltpu.roll(two, HEAD, 1)).astype(jnp.bfloat16)
+        values = jnp.where(lane < HEAD, pltpu.roll(one, HEAD, 1), two)
+        for k in range(2):
+            kv[half, ROWS + 128 * k : ROWS + 128 * (k + 1), :] = jnp.transpose(
+                values[128 * k : 128 * (k + 1)]
+            ).astype(jnp.bfloat16)
+        row_scale = lax.rsqrt(jnp.sum(jnp.transpose(square), axis=0, keepdims=True) / width + epsilon)
+        shared = acc_slim[SLIM[2] : SLIM[3], here] * row_scale
+        shared = turned(shared, ROPE // 2, slim_cos[:, here], slim_sin[:, here])
+        shared = jnp.concatenate(shared, axis=0)
+        groups = jnp.transpose(jnp.concatenate([shared[:, 0:128], shared[:, 128:256]] * 2, axis=0))
+        packed = jnp.where(lane[0:64] < 64, groups[0:64], groups[64:128])
+        kv[half, 2 * ROWS :, :] = packed.astype(jnp.bfloat16)
+        send_kv(half)
+
+    def make_q(half):
+        here = slice(half * ROWS, (half + 1) * ROWS)
+        total = jnp.sum(jnp.transpose(squares[here, :]), axis=0, keepdims=True)
+        part = acc_slim[0 : SLIM[0], here] * lax.rsqrt(total / width + epsilon)
+        wide = NOPE + ROPE
+        pieces = [part[0:NOPE], part[wide : wide + NOPE]]
+        for h in range(2):
+            pieces += turned(
+                part[wide * h + NOPE : wide * (h + 1)], ROPE // 2, slim_cos[:, here], slim_sin[:, here]
+            )
+        sharp = LOG2E * (NOPE + ROPE) ** (-0.5)
+        q[:, here] = (jnp.concatenate(pieces, axis=0) * sharp).astype(jnp.bfloat16)
+        send_q(half)
+
+    to_side(0, True).wait_recv()
+    onward(0, True).start()
+    to_side(1, False).wait_recv()
+    onward(0, False).start()
+    to_side(3, True).start()
+    to_side(2, False).start()
+    over(0, 0).wait_recv()
+    add(0, 0)
+    to_side(1, True).wait_recv()
+    over(1, 0).start()
+    to_side(0, False).wait_recv()
+    over(3, 0).start()
+    over(1, 0).wait_recv()
+    add(1, 0)
+    over(3, 0).wait_recv()
+    add(3, 0)
+    to_side(2, True).wait_recv()
+    onward(1, True).start()
+    to_side(3, False).wait_recv()
+    onward(1, False).start()
+    onward(0, True).wait_recv()
+    onward(0, False).wait_recv()
+    over(2, 0).start()
+    over(0, 1).wait_recv()
+    add(0, 1)
+    over(2, 0).wait_recv()
+    add(2, 0)
+    raise_ready()
+    make_kv(0)
+    make_q(0)
+    to_side(3, True).wait_recv()
+    over(1, 1).start()
+    to_side(2, False).wait_recv()
+    over(3, 1).start()
+    over(1, 1).wait_recv()
+    add(1, 1)
+    over(3, 1).wait_recv()
+    add(3, 1)
+    onward(1, True).wait_recv()
+    onward(1, False).wait_recv()
+    over(2, 1).start()
+    over(2, 1).wait_recv()
+    add(2, 1)
+    scale = lax.rsqrt(jnp.sum(squares[...], axis=1, keepdims=True) / width + epsilon)
+    row_scale = lax.rsqrt(jnp.sum(jnp.transpose(squares[...]), axis=0, keepdims=True) / width + epsilon)
     mixed = acc_slim[0 : SLIM[2]] * row_scale
     keys = jnp.concatenate(turned(mixed[SLIM[0] : SLIM[1]], HEAD // 2, wide_cos, wide_sin), axis=0)
     values_t = mixed[SLIM[1] : SLIM[2]]
     wkv[...] = jnp.transpose(jnp.concatenate([keys, values_t], axis=0)).astype(jnp.bfloat16)
     send_w()
-    sharp = LOG2E * (NOPE + ROPE) ** (-0.5)
-    wide = NOPE + ROPE
-    pieces = [mixed[0:NOPE], mixed[wide : wide + NOPE]]
-    for h in range(2):
-        pieces += turned(mixed[wide * h + NOPE : wide * (h + 1)], ROPE // 2, slim_cos, slim_sin)
-    q[...] = (jnp.concatenate(pieces, axis=0) * sharp).astype(jnp.bfloat16)
-    send_q()
-    raise_ready()
-    low = acc_ld[...] * scale
-    low = low * lax.rsqrt(jnp.mean(low * low, axis=1, keepdims=True) + epsilon) * lgain_ref[0:1, :]
-    expanded = jnp.dot(low.astype(jnp.bfloat16), up[...], preferred_element_type=jnp.float32)
-    lane = lax.broadcasted_iota(jnp.int32, (BLK, 128), 1)
-    one, two = expanded[:, 0:128], expanded[:, 128:256]
-    kv[0:BLK, :] = jnp.where(lane < HEAD, one, pltpu.roll(two, HEAD, 1)).astype(jnp.bfloat16)
-    values = jnp.where(lane < HEAD, pltpu.roll(one, HEAD, 1), two)
-    for k in range(4):
-        block = slice(BLK + 128 * k, BLK + 128 * (k + 1))
-        kv[block, :] = jnp.transpose(values[128 * k : 128 * (k + 1)]).astype(jnp.bfloat16)
-    shared = acc_slim[SLIM[2] : SLIM[3]] * row_scale
-    shared = jnp.concatenate(turned(shared, ROPE // 2, slim_cos, slim_sin), axis=0)
-    packed = jnp.concatenate([shared[:, 128 * k : 128 * (k + 1)] for k in range(4)], axis=0)
-    kv[2 * BLK :, :] = jnp.transpose(packed).astype(jnp.bfloat16)
-    send_kv()
+    make_kv(1)
+    make_q(1)
     queries = jnp.transpose(acc_wq[...] * scale)
     pieces = []
     for h in range(2):
         pieces += turned(queries[HEAD * h : HEAD * (h + 1)], HEAD // 2, wide_cos, wide_sin)
     wq[...] = (jnp.concatenate(pieces, axis=0) * (LOG2E * HEAD ** (-0.5))).astype(jnp.bfloat16)
 
-    sent = [own_over, onward(True), onward(False)]
-    sent += [to_side(half, way) for half in range(2) for way in (True, False)]
-    sent += [over(r, half) for r in (1, 2, 3) for half in range(2)]
+    sent = [to_side(quarter, way) for quarter in range(4) for way in (True, False)]
+    sent += [onward(half, way) for half in range(2) for way in (True, False)]
+    sent += [over(r, half) for r in range(X) for half in range(2)]
     return sent
 
 
@@ -355,7 +391,6 @@
     a_slim,
     a_ld,
     a_wq,
-    kv_ref,
     q_ref,
     wkv_ref,
     wq_ref,
@@ -367,6 +402,12 @@
     wkv,
     s0,
     s1,
+    s2,
+    s3,
+    s4,
+    s5,
+    s6,
+    s7,
     now_max,
     now_shrink,
     run_max,
@@ -420,8 +461,6 @@
         pltpu.make_async_copy(source, target, load_sem.at[n])
         for n, (source, target) in enumerate(zip(sources, targets))
     ]
-    for load in loads:
-        load.start()
     load_x.wait()
     pl.semaphore_wait(barrier, len(peers))
 
@@ -435,27 +474,47 @@
             device_id_type=MESH,
         )
 
-    def kv_half(ref, half):
-        return ref.at[pl.ds(half * HALF, HALF)]
-
     def kv_copy(step, half, upward):
         came = 0 if step == 1 else (2 * step - 3 if upward else 2 * step - 2)
-        goes = 7 if step == 4 else (2 * step - 1 if upward else 2 * step)
-        src = kv_half(kv_ref if step == 1 else kvs.at[came], half)
+        goes = 2 * step - 1 if upward else 2 * step
         slot = 2 * goes + half
         return copy(
-            src, kv_half(kvs.at[goes], half), kv_send.at[slot], kv_recv.at[slot], up if upward else down
-        )
-
-    q_half = q_ref.shape[0] // 2
-    q_right = copy(q_ref, qraw.at[1], q_send.at[0], q_recv.at[0], right)
-    q_left = copy(q_ref, qraw.at[2], q_send.at[1], q_recv.at[1], left)
-    q_on_right = copy(
-        qraw.at[1, pl.ds(0, q_half)], qraw.at[3, pl.ds(0, q_half)], q_send.at[2], q_recv.at[2], right
-    )
-    q_on_left = copy(
-        qraw.at[2, pl.ds(q_half, q_half)], qraw.at[3, pl.ds(q_half, q_half)], q_send.at[3], q_recv.at[3], left
-    )
+            kvs.at[came, half], kvs.at[goes, half], kv_send.at[slot], kv_recv.at[slot], up if upward else down
+        )
+
+    def kv_last(half, upward):
+        quarter = pl.ds(0 if upward else HALF // 2, HALF // 2)
+        slot = 14 + 2 * half + (0 if upward else 1)
+        return copy(
+            kvs.at[5 if upward else 6, half, quarter],
+            kvs.at[7, half, quarter],
+            kv_send.at[slot],
+            kv_recv.at[slot],
+            up if upward else down,
+        )
+
+    def q_side(half, rightward):
+        cols = pl.ds(half * ROWS, ROWS)
+        tag = half + (0 if rightward else 2)
+        return copy(
+            q_ref.at[:, cols],
+            qraw.at[1 if rightward else 2, :, cols],
+            q_send.at[tag],
+            q_recv.at[tag],
+            right if rightward else left,
+        )
+
+    def q_onward(rightward):
+        cols = pl.ds(0 if rightward else ROWS, ROWS)
+        tag = 4 if rightward else 5
+        return copy(
+            qraw.at[1 if rightward else 2, :, cols],
+            qraw.at[3, :, cols],
+            q_send.at[tag],
+            q_recv.at[tag],
+            right if rightward else left,
+        )
+
     w_after = copy(
         wkv_ref.at[pl.ds(BLK - WINDOW, WINDOW)], wkv.at[pl.ds(0, WINDOW)], w_send.at[0], w_recv.at[0], after
     )
@@ -464,21 +523,20 @@
     )
 
     def load_weights():
+        for load in loads:
+            load.start()
         run_max[...] = jnp.full(run_max.shape, -1e30, jnp.float32)
         acc[...] = jnp.zeros(acc.shape, jnp.float32)
         for load in loads[:-3]:
             load.wait()
 
-    def send_kv():
-        for load in loads[-2:]:
-            load.wait()
-        for half in range(2):
-            kv_copy(1, half, True).start()
-            kv_copy(1, half, False).start()
-
-    def send_q():
-        q_right.start()
-        q_left.start()
+    def send_kv(half):
+        kv_copy(1, half, True).start()
+        kv_copy(1, half, False).start()
+
+    def send_q(half):
+        q_side(half, True).start()
+        q_side(half, False).start()
 
     def send_w():
         w_after.start()
@@ -491,7 +549,7 @@
         far_ref,
         (w_slim, w_ld, w_wq),
         w_up,
-        kv_ref,
+        kvs.at[0],
         q_ref,
         wkv_ref,
         wq_ref,
@@ -507,7 +565,7 @@
         send_w,
     )
 
-    scores_of = (s0, s1)
+    tiles = (s0, s1, s2, s3, s4, s5, s6, s7)
     blank = jnp.zeros((NOPE, BLK), jnp.bfloat16)
 
     def set_queries(g, src):
@@ -520,32 +578,46 @@
             qpad[2 * g + h, 2 * NOPE : 2 * NOPE + ROPE] = src[start : start + ROPE, :]
             qpad[2 * g + h, 2 * NOPE + ROPE :] = jnp.zeros((128 - ROPE, BLK), jnp.bfloat16)
 
-    def set_ropes(p, packed):
-        wide = packed.astype(jnp.float32)
-        ropes[p, 0:128] = packed
-        for k in range(1, 4):
-            ropes[p, 128 * k : 128 * (k + 1)] = pltpu.roll(wide, 128 - 32 * k, 1).astype(jnp.bfloat16)
+    def set_ropes(p):
+        for half in range(2):
+            packed = kvs[p, half, 2 * ROWS :, :]
+            wide = packed.astype(jnp.float32)
+            start = half * ROWS
+            ropes[p, start : start + 64] = packed
+            for k, shift in enumerate((64, 96, 32)):
+                turned_keys = pltpu.roll(wide, shift, 1).astype(jnp.bfloat16)
+                ropes[p, start + 64 * (k + 1) : start + 64 * (k + 2)] = turned_keys
 
     def keys_of(p):
-        return jnp.concatenate([kvs[p, 0:BLK, :], ropes[p]], axis=1)
-
-    def scores_stage(p, g, h):
-        scores = jnp.dot(keys_of(p), qpad[2 * g + h], preferred_element_type=jnp.float32)
-        scores_of[h][...] = scores
-        before_max = run_max[2 * g + h]
+        keys = jnp.concatenate([kvs[p, 0, 0:ROWS, :], kvs[p, 1, 0:ROWS, :]], axis=0)
+        return jnp.concatenate([keys, ropes[p]], axis=1)
+
+    def scores_stage(unit, h, j, n):
+        p, g = unit
+        cols = slice(n * TILE, (n + 1) * TILE)
+        scores = jnp.dot(keys_of(p), qpad[2 * g + h, :, cols], preferred_element_type=jnp.float32)
+        tiles[4 * h + 2 * j + n][...] = scores
+        before_max = run_max[2 * g + h, :, cols]
         highest = jnp.maximum(before_max, jnp.max(scores, axis=0, keepdims=True))
-        now_shrink[h] = jnp.exp2(before_max - highest)
-        now_max[h] = highest
-        run_max[2 * g + h] = highest
-
-    def values_stage(p, g, h):
-        weights = jnp.exp2(scores_of[h][...] - now_max[h]).astype(jnp.bfloat16)
+        now_shrink[2 * h + j, :, cols] = jnp.exp2(before_max - highest)
+        now_max[2 * h + j, :, cols] = highest
+        run_max[2 * g + h, :, cols] = highest
+
+    def values_stage(unit, h, j, n):
+        p, g = unit
+        cols = slice(n * TILE, (n + 1) * TILE)
+        weights = jnp.exp2(tiles[4 * h + 2 * j + n][...] - now_max[2 * h + j, :, cols]).astype(jnp.bfloat16)
         values = jnp.concatenate(
-            [kvs[p, pl.ds(BLK + 128 * k + HEAD * h, HEAD), :] for k in range(4)], axis=1
+            [
+                kvs[p, half, pl.ds(ROWS + 128 * k + HEAD * h, HEAD), :]
+                for half in range(2)
+                for k in range(2)
+            ],
+            axis=1,
         )
         values = jnp.concatenate([values, jnp.ones((16, BLK), jnp.bfloat16)], axis=0)
         mix = jnp.dot(values, weights, preferred_element_type=jnp.float32)
-        acc[2 * g + h] = acc[2 * g + h] * now_shrink[h] + mix
+        acc[2 * g + h, :, cols] = acc[2 * g + h, :, cols] * now_shrink[2 * h + j, :, cols] + mix
 
     def finish(g, h):
         total = acc[2 * g + h]
@@ -575,98 +647,100 @@
         g = jnp.where(u < 27, g, 0)
         return p, g
 
-    kvs[0] = kv_ref[...]
     set_queries(0, q_ref)
-    set_ropes(0, kv_ref[2 * BLK :, :])
+    set_ropes(0)
+    for load in loads[-2:]:
+        load.wait()
     wkv[WINDOW : WINDOW + BLK, :] = wkv_ref[...]
+    def arrive(step, half):
+        kv_copy(step, half, True).wait_recv()
+        kv_copy(step, half, False).wait_recv()
+
+    arrive(1, 0)
+    kv_copy(2, 0, True).start()
+    kv_copy(2, 0, False).start()
     w_after.wait_recv()
     w_before.wait_recv()
     window_part(wkv, wq_ref, sink_ref, out_ref, sp, length_all)
-    scores_stage(0, 0, 0)
-
-    def arrive(step, half):
-        kv_copy(step, half, True).wait_recv()
-        kv_copy(step, half, False).wait_recv()
+
+    q_side(0, True).wait_recv()
+    q_onward(True).start()
+    q_side(0, False).wait_recv()
+    q_side(1, False).wait_recv()
+    q_onward(False).start()
+    q_side(1, True).wait_recv()
+    set_queries(1, qraw.at[1])
+    set_queries(2, qraw.at[2])
+    parts = [(j, n) for j in range(2) for n in range(2)]
+    for j, n in parts:
+        scores_stage(unit(j), 0, j, n)
 
     def at0():
-        q_right.wait_recv()
-        q_on_right.start()
-        q_left.wait_recv()
-        q_on_left.start()
-        set_queries(1, qraw.at[1])
-        set_queries(2, qraw.at[2])
-
-    def at1():
-        arrive(1, 0)
-        kv_copy(2, 0, True).start()
-        kv_copy(2, 0, False).start()
-
-    def at2():
         arrive(1, 1)
         kv_copy(2, 1, True).start()
         kv_copy(2, 1, False).start()
-        set_ropes(1, kvs[1, 2 * BLK :, :])
-        set_ropes(2, kvs[2, 2 * BLK :, :])
-
-    def at5():
+        set_ropes(1)
+        set_ropes(2)
+
+    def at2():
         arrive(2, 0)
         kv_copy(3, 0, True).start()
         kv_copy(3, 0, False).start()
-
-    def at6():
-        q_on_right.wait_recv()
-        q_on_left.wait_recv()
+        q_onward(True).wait_recv()
+        q_onward(False).wait_recv()
         set_queries(3, qraw.at[3])
 
-    def at9():
+    def at4():
         arrive(2, 1)
         kv_copy(3, 1, True).start()
         kv_copy(3, 1, False).start()
-        set_ropes(3, kvs[3, 2 * BLK :, :])
-        set_ropes(4, kvs[4, 2 * BLK :, :])
+        set_ropes(3)
+        set_ropes(4)
+
+    def at6():
+        arrive(3, 0)
+        kv_last(0, True).start()
+        kv_last(0, False).start()
+
+    def at8():
+        arrive(3, 1)
+        kv_last(1, True).start()
+        kv_last(1, False).start()
+        set_ropes(5)
+        set_ropes(6)
+
+    def at11():
+        for half in range(2):
+            kv_last(half, True).wait_recv()
+            kv_last(half, False).wait_recv()
+        set_ropes(7)
 
     def at13():
-        arrive(3, 0)
-        kv_copy(4, 0, True).start()
-
-    def at17():
-        arrive(3, 1)
-        kv_copy(4, 1, False).start()
-        set_ropes(5, kvs[5, 2 * BLK :, :])
-        set_ropes(6, kvs[6, 2 * BLK :, :])
-
-    def at23():
-        kv_copy(4, 0, True).wait_recv()
-        kv_copy(4, 1, False).wait_recv()
-        set_ropes(7, kvs[7, 2 * BLK :, :])
-
-    events = {
-        0: at0,
-        1: at1,
-        2: at2,
-        5: at5,
-        6: at6,
-        9: at9,
-        13: at13,
-        17: at17,
-        23: at23,
-        25: lambda: send_out(3),
-        26: lambda: send_out(2),
-        27: lambda: send_out(1),
-    }
-
-    def advance(u, carry):
+        send_out(3)
+        send_out(2)
+
+    events = {0: at0, 2: at2, 4: at4, 6: at6, 8: at8, 11: at11, 13: at13, 14: lambda: send_out(1)}
+
+    def advance(i, carry):
         for when, event in events.items():
-            pl.when(u == when)(event)
-        p, g = unit(u)
-        p_next, g_next = unit(jnp.minimum(u + 1, 31))
-        scores_stage(p, g, 1)
-        values_stage(p, g, 0)
-        scores_stage(p_next, g_next, 0)
-        values_stage(p, g, 1)
+            pl.when(i == when)(event)
+        pair = [unit(2 * i), unit(2 * i + 1)]
+        following = [unit(2 * i + 2), unit(2 * i + 3)]
+        for j, n in parts:
+            scores_stage(pair[j], 1, j, n)
+            values_stage(pair[j], 0, j, n)
+        for j, n in parts:
+            scores_stage(following[j], 0, j, n)
+            values_stage(pair[j], 1, j, n)
         return carry
 
-    lax.fori_loop(0, 32, advance, 0)
+    lax.fori_loop(0, PAIRS - 1, advance, 0)
+    pair = [unit(2 * PAIRS - 2), unit(2 * PAIRS - 1)]
+    for j, n in parts:
+        scores_stage(pair[j], 1, j, n)
+        values_stage(pair[j], 0, j, n)
+    for j, n in parts:
+        values_stage(pair[j], 1, j, n)
 
     own = [finish(0, h) for h in range(2)]
     for g in range(1, 4):
@@ -690,11 +764,12 @@
         out_ref, w_ol, w_ow, result_ref, pair_out, pair_in, passed, gone, kept, side_out, side_in, r_send, r_recv
     )
 
-    w_sends = [w_after, w_before, q_right, q_left, q_on_right, q_on_left]
+    w_sends = [w_after, w_before, q_onward(True), q_onward(False)]
+    w_sends += [q_side(half, way) for half in range(2) for way in (True, False)]
     for step in range(1, 4):
         for half in range(2):
             w_sends += [kv_copy(step, half, True), kv_copy(step, half, False)]
-    w_sends += [kv_copy(4, 0, True), kv_copy(4, 1, False)]
+    w_sends += [kv_last(half, way) for half in range(2) for way in (True, False)]
     w_sends += [o_copy(g) for g in range(1, 4)]
     for sent in w_sends + x_sent + r_sent:
         sent.wait_send()
@@ -738,7 +813,7 @@
     rows = norm_gain.shape[0]
     return pl.pallas_call(
         functools.partial(layer_kernel, length_all),
-        out_shape=jax.ShapeDtypeStruct((BLK, COLS), bf16),
+        out_shape=pltpu.VMEM((BLK, COLS), bf16),
         in_specs=[in_smem] + [in_hbm] * 14,
         out_specs=in_vmem,
         scratch_shapes=[
@@ -757,20 +832,18 @@
             pltpu.VMEM((SLIM[3], BLK), f32),
             pltpu.VMEM((BLK, latent_down.shape[1]), f32),
             pltpu.VMEM((BLK, window_query.shape[1]), f32),
-            pltpu.VMEM((KV_ROWS, 128), bf16),
             pltpu.VMEM((2 * (NOPE + ROPE), BLK), bf16),
             pltpu.VMEM((BLK, 2 * HEAD), bf16),
             pltpu.VMEM((2 * HEAD, BLK), bf16),
             pltpu.VMEM((BLK, 4 * HEAD), bf16),
-            pltpu.VMEM((Z, KV_ROWS, 128), bf16),
+            pltpu.VMEM((Z, 2, HALF, 128), bf16),
             pltpu.VMEM((Z, BLK, 128), bf16),
             pltpu.VMEM((Y, 2 * (NOPE + ROPE), BLK), bf16),
             pltpu.VMEM((2 * Y, 256, BLK), bf16),
             pltpu.VMEM((BLK + 2 * WINDOW, 128), bf16),
-            pltpu.VMEM((BLK, BLK), f32),
-            pltpu.VMEM((BLK, BLK), f32),
-            pltpu.VMEM((2, 1, BLK), f32),
-            pltpu.VMEM((2, 1, BLK), f32),
+            *[pltpu.VMEM((BLK, TILE), f32)] * 8,
+            pltpu.VMEM((4, 1, BLK), f32),
+            pltpu.VMEM((4, 1, BLK), f32),
             pltpu.VMEM((2 * Y, 1, BLK), f32),
             pltpu.VMEM((2 * Y, HEAD + 16, BLK), f32),
             pltpu.VMEM((Y - 1, O_ROWS, BLK), bf16),
@@ -783,12 +856,12 @@
             pltpu.VMEM((4, ROWS, COLS), bf16),
             pltpu.VMEM((4, ROWS, COLS), bf16),
             dma((14,)),
-            dma((16,)),
-            dma((16,)),
-            dma((16,)),
-            dma((16,)),
-            dma((4,)),
-            dma((4,)),
+            dma((20,)),
+            dma((20,)),
+            dma((18,)),
+            dma((18,)),
+            dma((6,)),
+            dma((6,)),
             dma((3,)),
             dma((3,)),
             dma((2,)),

time: 77 us -> 72.5 us (0.942)
  Pallas kernels: 75.2 us -> 71.5 us
  local copies, waits for them, and re-layouts: 1.67 us -> 0.71 us
    pallas_call x1, Pallas kernels: 75.2 us -> 71.5 us  [shards(): pl.pallas_call(functools.partial(layer_kernel, length_all), out_shape=plt...]
    unnamed x1, local copies, waits for them, and re-layouts: 1.67 us -> 0.71 us
where the time goes in v3:
time: 72.5 us; the launch traced here: 72.2 us
  Pallas kernels  71.5 us (99%)
    pallas_call x1, Pallas kernels, shards(): pl.pallas_call(functools.partial(layer_kernel, length_all), out_shape=plt...  71.5 us

profile of v3, /device:TPU:1, one launch (start us, length us, event | category | flops | bytes accessed | tf_op | source)
XLA Modules:
  0.0 72.2 jit_solution(201762230206098351)
XLA Ops:
  0.0 71.5 %layer.1 = bf16[512,256]{1,0:T(8,128)(2,1)S(1)} custom-call(f32[2]{0:T(128)} %sink_ref.1, bf16[512,256]{1,0:T(8,128)(2,1)} %x_hbm.1, f32[1,2048]{1,0:T(1,128)} %bitcast.10, f32[1,512]{1,0:T(1,128)} %bitcast.11, f32[2,48,512]{2,1,0:T(8,128)} %constant.4.clone.near_hbm, f32[2,48,128]{2,1,0:T(8,128)} %constant.5.clone.far_hbm, bf16[192,2048]{1,0:T(8,128)(2,1)} %bitcast.6, ...), custom_call_target="tpu_custom_call" | custom-call | tf_op jit(solution)/shard_map/layer/pallas_call | solution.py:814
  71.5 0.7 copy.17

commit v4 on v3

--- a/solution.py
+++ b/solution.py
@@ -286,14 +286,18 @@
     partner = 2 * x + 1 - core
     values = mixed[...]
 
-    def projected(r, core_to):
+    def projected(r, core_to, half):
         block = ((x + r) % X) * 2 + core_to
         cols = pl.ds(pl.multiple_of(block * COLS, COLS), COLS)
         weight = jnp.concatenate([wl[:, cols], ww[:, cols]], axis=0)
-        return jnp.dot(values, weight, preferred_element_type=jnp.float32)
-
-    def pair(r):
-        return remote(pair_out.at[r], pair_in.at[r], r_send.at[r], r_recv.at[r], at_tp(partner))
+        return jnp.dot(values[half * ROWS : (half + 1) * ROWS], weight, preferred_element_type=jnp.float32)
+
+    def pair(r, half):
+        rows = pl.ds(half * ROWS, ROWS)
+        tag = 6 + 2 * r + half + 4
+        return remote(
+            pair_out.at[r, rows], pair_in.at[r, rows], r_send.at[tag], r_recv.at[tag], at_tp(partner)
+        )
 
     def far(half):
         return remote(
@@ -307,23 +311,29 @@
         )
 
     def start_pair(r):
-        pair_out[r] = projected(r, 1 - core).astype(jnp.bfloat16)
-        pair(r).start()
+        for half in range(2):
+            rows = slice(half * ROWS, (half + 1) * ROWS)
+            pair_out[r, rows] = projected(r, 1 - core, half).astype(jnp.bfloat16)
+            pair(r, half).start()
+
+    def total_of(r, half, own):
+        pair(r, half).wait_recv()
+        return own + pair_in[r, half * ROWS : (half + 1) * ROWS].astype(jnp.float32)
 
     order = (2, 1, 3, 0)
     start_pair(2)
-    own_next = projected(2, core)
+    own_next = [projected(2, core, half) for half in range(2)]
     start_pair(1)
     for n, r in enumerate(order):
         own = own_next
-        pair(r).wait_recv()
-        total = own + pair_in[r].astype(jnp.float32)
-        upper, lower = total[:ROWS], total[ROWS:]
         if r == 2:
-            gone[0] = upper.astype(jnp.bfloat16)
-            far(0).start()
-            gone[1] = lower.astype(jnp.bfloat16)
-            far(1).start()
+            for half in range(2):
+                gone[half] = total_of(r, half, own[half]).astype(jnp.bfloat16)
+                far(half).start()
+        else:
+            upper, lower = total_of(r, 0, own[0]), total_of(r, 1, own[1])
+        if r == 2:
+            pass
         elif r == 1:
             side_out[1] = lower.astype(jnp.bfloat16)
             side(True, 1).start()
@@ -338,7 +348,7 @@
         if n < 2:
             start_pair(order[n + 2])
         if n < 3:
-            own_next = projected(order[n + 1], core)
+            own_next = [projected(order[n + 1], core, half) for half in range(2)]
     far(0).wait_recv()
     side_out[0] = (kept[0] + passed[0].astype(jnp.float32)).astype(jnp.bfloat16)
     side(True, 0).start()
@@ -351,7 +361,7 @@
     for half in range(2):
         total = kept[2 + half] + side_in[half].astype(jnp.float32) + side_in[2 + half].astype(jnp.float32)
         out_ref[half * ROWS : (half + 1) * ROWS, :] = total.astype(jnp.bfloat16)
-    sent = [pair(r) for r in range(X)] + [far(half) for half in range(2)]
+    sent = [pair(r, half) for r in range(X) for half in range(2)] + [far(half) for half in range(2)]
     return sent + [side(way, half) for way in (True, False) for half in range(2)]
 
 
@@ -866,8 +876,8 @@
             dma((3,)),
             dma((2,)),
             dma((2,)),
-            dma((10,)),
-            dma((10,)),
+            dma((18,)),
+            dma((18,)),
         ],
         compiler_params=pltpu.CompilerParams(
             collective_id=1, has_side_effects=True, vmem_limit_bytes=VMEM_LIMIT

time: 72.5 us -> 73.3 us (1.011)
  no operation moved by 1% of the time
where the time goes in v4:
time: 73.3 us; the launch traced here: 72.7 us
  Pallas kernels  72 us (98%)
    pallas_call x1, Pallas kernels, shards(): pl.pallas_call(functools.partial(layer_kernel, length_all), out_shape=plt...  72 us

profile of v4, /device:TPU:1, one launch (start us, length us, event | category | flops | bytes accessed | tf_op | source)
XLA Modules:
  0.0 72.7 jit_solution(17301080709782743960)
XLA Ops:
  0.0 72.0 %layer.1 = bf16[512,256]{1,0:T(8,128)(2,1)S(1)} custom-call(f32[2]{0:T(128)} %sink_ref.1, bf16[512,256]{1,0:T(8,128)(2,1)} %x_hbm.1, f32[1,2048]{1,0:T(1,128)} %bitcast.10, f32[1,512]{1,0:T(1,128)} %bitcast.11, f32[2,48,512]{2,1,0:T(8,128)} %constant.4.clone.near_hbm, f32[2,48,128]{2,1,0:T(8,128)} %constant.5.clone.far_hbm, bf16[192,2048]{1,0:T(8,128)(2,1)} %bitcast.6, ...), custom_call_target="tpu_custom_call" | custom-call | tf_op jit(solution)/shard_map/layer/pallas_call | solution.py:824
  72.0 0.7 copy.17
